TPU v7x, 32 devices: a whole 2x2x4 slice. The times are simulated.
32 devices in a mesh: dp: 4 (over y, x), kv: 4 (over z), tp: 2 (over core).
Axes of the slice: x: 2, y: 2, z: 4, core: 2. Of those that a mesh axis runs over, the one named last changes fastest.
Arguments:
- tokens: bfloat16 [32, 2048], P('dp', ('kv', 'tp')), parts along dimension 0, may hold values from -8 to 8
- mlp1_gain: float32 [2048], replicated, may hold values from 0.1 to 1.9
- mlp1_gate: bfloat16 [2048, 5632], P(None, ('kv', 'tp')), may hold values from -0.125 to 0.125
- mlp1_up: bfloat16 [2048, 5632], P(None, ('kv', 'tp')), may hold values from -0.125 to 0.125
- mlp1_down: bfloat16 [5632, 2048], P(('kv', 'tp')), may hold values from -0.109375 to 0.109375
- mixer_gain: float32 [2048], replicated, may hold values from 0.1 to 1.9
- proj_z: bfloat16 [2048, 2048], P('kv', 'tp'), may hold values from -0.125 to 0.125
- proj_x: bfloat16 [2048, 2048], P('kv', 'tp'), may hold values from -0.125 to 0.125
- proj_bc: bfloat16 [2048, 2, 512], P('kv', None, 'tp'), may hold values from -0.125 to 0.125
- proj_dt: bfloat16 [2048, 32], P('kv', 'tp'), may hold values from -0.125 to 0.125
- conv_x: bfloat16 [4, 2048], P(None, 'tp'), may hold values from -3 to 3
- conv_bc: bfloat16 [4, 2, 512], P(None, None, 'tp'), may hold values from -3 to 3
- window_x: bfloat16 [32, 3, 2048], P(('dp', 'kv'), None, 'tp'), parts along dimension 0, may hold values from -6 to 6
- window_bc: bfloat16 [32, 3, 2, 512], P(('dp', 'kv'), None, None, 'tp'), parts along dimension 0, may hold values from -6 to 6
- ssm_state: float32 [32, 32, 64, 128], P(('dp', 'kv'), 'tp'), parts along dimension 0, may hold values from -0.8 to 0.8
- dt_bias: float32 [32], P('tp'), may hold values from -4 to 0
- log_rate: float32 [32], P('tp'), may hold values from 0 to 2.77
- skip_gain: float32 [32], P('tp'), may hold values from 0.25 to 2
- group_gain: float32 [2048], P('tp'), may hold values from 0.1 to 1.9
- out_weight: bfloat16 [2048, 2048], P('tp', 'kv'), may hold values from -0.125 to 0.125
- mlp2_gain: float32 [2048], replicated, may hold values from 0.1 to 1.9
- mlp2_gate: bfloat16 [2048, 5632], P(None, ('kv', 'tp')), may hold values from -0.125 to 0.125
- mlp2_up: bfloat16 [2048, 5632], P(None, ('kv', 'tp')), may hold values from -0.125 to 0.125
- mlp2_down: bfloat16 [5632, 2048], P(('kv', 'tp')), may hold values from -0.109375 to 0.109375
Outputs:
- result: bfloat16 [32, 2048], P('dp', ('kv', 'tp')), parts along dimension 0
- new_state: float32 [32, 32, 64, 128], P(('dp', 'kv'), 'tp'), parts along dimension 0
- new_window_x: bfloat16 [32, 3, 2048], P(('dp', 'kv'), None, 'tp'), parts along dimension 0
- new_window_bc: bfloat16 [32, 3, 2, 512], P(('dp', 'kv'), None, None, 'tp'), parts along dimension 0
There are 4 independent parts, one for each index of `dp`. A program takes and returns all parts, laid end to end along the dimension named above; an argument that names none is the same for every part. Nothing has to cross between parts.
All inputs are finite; a program needn't handle non-finite values.
Results may differ from a plain program's by a relative error of at most 0.013.
Values may be sent and summed in bfloat16 or wider, within the bound.
A program may use at most 64 MiB of HBM per device.

v0:
```python
import jax
import jax.numpy as jnp
from jax import lax
from jax.sharding import PartitionSpec as P

EPS = 1e-06


def norm_rows(values, scale_gain):
    floats = values.astype(jnp.float32)
    factor = lax.rsqrt(jnp.mean(floats * floats, axis=-1, keepdims=True) + EPS)
    return (floats * factor * scale_gain).astype(jnp.bfloat16)


def half_mlp(columns, scale_gain, gate_weight, up_weight, down_weight):
    gathered = lax.all_gather(columns, ("kv", "tp"), axis=1, tiled=True)
    normed = norm_rows(gathered, scale_gain)
    gate_part = jnp.dot(normed, gate_weight, preferred_element_type=jnp.float32)
    up_part = jnp.dot(normed, up_weight, preferred_element_type=jnp.float32)
    hidden = (jax.nn.silu(gate_part) * up_part).astype(jnp.bfloat16)
    partial_sums = jnp.dot(hidden, down_weight, preferred_element_type=jnp.float32)
    summed = lax.psum_scatter(partial_sums, ("kv", "tp"), scatter_dimension=1, tiled=True)
    return (columns.astype(jnp.float32) + 0.5 * summed).astype(jnp.bfloat16)


def per_device(
    tokens,
    mlp1_gain,
    mlp1_gate,
    mlp1_up,
    mlp1_down,
    mixer_gain,
    proj_z,
    proj_x,
    proj_bc,
    proj_dt,
    conv_x,
    conv_bc,
    window_x,
    window_bc,
    ssm_state,
    dt_bias,
    log_rate,
    skip_gain,
    group_gain,
    out_weight,
    mlp2_gain,
    mlp2_gate,
    mlp2_up,
    mlp2_down,
):
    after_first = half_mlp(tokens, mlp1_gain, mlp1_gate, mlp1_up, mlp1_down)
    kv_width = proj_z.shape[0]
    kv_offset = lax.axis_index("kv") * kv_width
    gathered = lax.all_gather(after_first, ("kv", "tp"), axis=1, tiled=True)
    floats = gathered.astype(jnp.float32)
    squares = jnp.sum(floats * floats, axis=1)
    own_cols = lax.dynamic_slice_in_dim(gathered, kv_offset, kv_width, 1)
    model_width = kv_width * lax.axis_size("kv")
    factor = lax.rsqrt(squares / model_width + EPS)
    gain_cols = lax.dynamic_slice_in_dim(mixer_gain, kv_offset, kv_width, 0)
    normed = (own_cols.astype(jnp.float32) * factor[:, None] * gain_cols).astype(jnp.bfloat16)
    inner_width = proj_z.shape[1]
    group_width = proj_bc.shape[2]
    joined = jnp.concatenate(
        [proj_z, proj_x, proj_bc.reshape(kv_width, 2 * group_width), proj_dt], axis=1
    )
    own_seqs = window_x.shape[0]
    projected = lax.psum_scatter(
        jnp.dot(normed, joined, preferred_element_type=jnp.float32),
        "kv",
        scatter_dimension=0,
        tiled=True,
    )
    gate_z = projected[:, :inner_width].astype(jnp.bfloat16)
    x_new = projected[:, inner_width : 2 * inner_width].astype(jnp.bfloat16)
    bc_end = 2 * inner_width + 2 * group_width
    bc_new = (
        projected[:, 2 * inner_width : bc_end]
        .astype(jnp.bfloat16)
        .reshape(own_seqs, 2, group_width)
    )
    rate_raw = projected[:, bc_end:]
    full_x = jnp.concatenate([window_x, x_new[:, None]], axis=1)
    full_bc = jnp.concatenate([window_bc, bc_new[:, None]], axis=1)
    mixed_x = jax.nn.silu(
        jnp.einsum("sji,ji->si", full_x.astype(jnp.float32), conv_x.astype(jnp.float32))
    )
    mixed_bc = jax.nn.silu(
        jnp.einsum("sjci,jci->sci", full_bc.astype(jnp.float32), conv_bc.astype(jnp.float32))
    )
    heads = proj_dt.shape[1]
    state_size = ssm_state.shape[3]
    groups = group_width // state_size
    head_dim = inner_width // heads
    repeat = heads // groups
    inputs_x = mixed_x.reshape(own_seqs, heads, head_dim)
    keys_b = jnp.repeat(mixed_bc[:, 0].reshape(own_seqs, groups, state_size), repeat, axis=1)
    reads_c = jnp.repeat(mixed_bc[:, 1].reshape(own_seqs, groups, state_size), repeat, axis=1)
    step_size = jax.nn.softplus(rate_raw + dt_bias)
    retain = jnp.exp(-step_size * jnp.exp(log_rate))
    new_state = (
        retain[:, :, None, None] * ssm_state
        + (step_size[:, :, None] * inputs_x)[:, :, :, None] * keys_b[:, :, None, :]
    )
    readout = jnp.einsum("shpn,shn->shp", new_state, reads_c) + skip_gain[None, :, None] * inputs_x
    gated = readout.reshape(own_seqs, inner_width) * jax.nn.silu(gate_z.astype(jnp.float32))
    grouped = gated.reshape(own_seqs, groups, inner_width // groups)
    grouped = grouped * lax.rsqrt(jnp.mean(grouped * grouped, axis=-1, keepdims=True) + EPS)
    mixed = (grouped.reshape(own_seqs, inner_width) * group_gain).astype(jnp.bfloat16)
    partial_out = jnp.dot(
        lax.all_gather(mixed, "kv", axis=0, tiled=True),
        out_weight,
        preferred_element_type=jnp.float32,
    )
    summed_out = lax.psum_scatter(
        partial_out.astype(jnp.bfloat16), "tp", scatter_dimension=1, tiled=True
    ).astype(jnp.float32)
    after_mixer = (after_first.astype(jnp.float32) + summed_out).astype(jnp.bfloat16)
    result = half_mlp(after_mixer, mlp2_gain, mlp2_gate, mlp2_up, mlp2_down)
    return (result, new_state, full_x[:, 1:], full_bc[:, 1:])


def solution(mesh):
    placed = (
        P("dp", ("kv", "tp")),
        P(),
        P(None, ("kv", "tp")),
        P(None, ("kv", "tp")),
        P(("kv", "tp"), None),
        P(),
        P("kv", "tp"),
        P("kv", "tp"),
        P("kv", None, "tp"),
        P("kv", "tp"),
        P(None, "tp"),
        P(None, None, "tp"),
        P(("dp", "kv"), None, "tp"),
        P(("dp", "kv"), None, None, "tp"),
        P(("dp", "kv"), "tp", None, None),
        P("tp"),
        P("tp"),
        P("tp"),
        P("tp"),
        P("tp", "kv"),
        P(),
        P(None, ("kv", "tp")),
        P(None, ("kv", "tp")),
        P(("kv", "tp"), None),
    )
    return jax.shard_map(
        per_device,
        mesh=mesh,
        in_specs=placed,
        out_specs=(
            P("dp", ("kv", "tp")),
            P(("dp", "kv"), "tp", None, None),
            P(("dp", "kv"), None, "tp"),
            P(("dp", "kv"), None, None, "tp"),
        ),
        check_vma=False,
    )
```

profile of v0, /device:TPU:0, one launch (start us, length us, event | category | flops | bytes accessed | tf_op | source)
XLA Modules:
  0.0 202.9 jit_solution(11177478440627471984)
XLA Ops:
  7.2 0.0 copy-start
  7.2 0.0 copy-start.4
  7.2 0.0 reduce-scatter.4.cloned.1.call-start
  7.2 16.1 %all_gather.12 = bf16[8,2048]{1,0:T(8,128)(2,1)S(1)} all-gather(bf16[8,256]{1,0:T(8,128)(2,1)} %param.24), channel_id=1, replica_groups=mesh['dp'=4,'kv'=4,'tp'=2] {'kv','tp'}, dimensions={1}, use_global_device_ids=true | all-gather | bytes 36864 | tf_op jit(solution)/shard_map/all_gather | solution.py:16
  23.3 0.1 fusion.12
  23.4 2.7 %fusion.46 = f32[8,704]{1,0:T(8,128)S(1)} fusion(bf16[2048,704]{0,1:T(8,128)(2,1)} %param.26, bf16[8,2048]{1,0:T(8,128)(2,1)S(1)} %all_gather.12, f32[2048]{0:T(1024)} %param.25, f32[8]{0:T(128)S(1)} %add_rsqrt_fusion.3), kind=kOutput, calls=%fused_computation.70 | convolution fusion | flops 23134208 | bytes 2947104 | tf_op jit(solution)/shard_map/dot_general | solution.py:18
  26.1 0.0 copy-done
  26.1 0.0 copy-done.4
  26.1 0.0 copy-start.2
  26.1 0.0 copy-start.7
  26.2 0.0 copy-start.9
  26.2 0.0 copy-start.8
  26.2 4.1 %fusion.11 = f32[8,2048]{1,0:T(8,128)} fusion(bf16[704,2048]{1,0:T(8,128)(2,1)S(1)} %copy-done, bf16[2048,704]{0,1:T(8,128)(2,1)} %param.27, f32[8,704]{1,0:T(8,128)S(1)} %fusion.46, bf16[8,2048]{1,0:T(8,128)(2,1)S(1)} %all_gather.12, f32[2048]{0:T(1024)S(1)} %copy-done.4, f32[8]{0:T(128)S(1)} %add_rsqrt_fusion.3), kind=kOutput, calls=%fused_computation.13 | convolution fusion | flops 46236672 | bytes 5896224 | tf_op jit(solution)/shard_map/dot_general | solution.py:21
  30.3 0.0 reduce-scatter.4.cloned.1.call-update
  30.3 0.0 all-reduce.3.cloned.1.call-start
  30.4 0.0 copy-done.2
  30.4 0.9 copy.51
  31.3 0.0 copy-done.7
  31.3 0.1 copy.30
  31.4 0.8 dynamic_slice.7
  32.2 0.0 copy-done.9
  32.2 29.8 %reduce-scatter.4.cloned.1.call-done = f32[8,256]{1,0:T(8,128)} async-done(((f32[8,2048]{1,0:T(8,128)}), f32[8,256]{1,0:T(8,128)}) %reduce-scatter.4.cloned.1.call-update) | async-done | bytes 8208 | tf_op jit(solution)/shard_map/reduce_scatter | solution.py:22
  62.0 0.7 add_convert_fusion.2
  62.7 14.1 %all_gather.13 = bf16[8,2048]{1,0:T(8,128)(2,1)S(1)} all-gather(bf16[8,256]{1,0:T(8,128)(2,1)S(1)} %add_convert_fusion.2), channel_id=1, replica_groups=mesh['dp'=4,'kv'=4,'tp'=2] {'kv','tp'}, dimensions={1}, use_global_device_ids=true | all-gather | bytes 36864 | tf_op jit(solution)/shard_map/all_gather | solution.py:55
  76.8 0.1 multiply_reduce_fusion
  76.9 0.0 copy-start.14
  76.9 0.0 copy-start.15
  76.9 0.0 copy-start.3
  76.9 0.0 copy-start.6
  77.0 0.0 copy-start.13
  77.0 2.9 %fusion = f32[8,2576]{1,0:T(8,128)} fusion(bf16[512,16]{1,0:T(8,128)(2,1)S(1)} %copy.30, bf16[512,512]{1,0:T(8,128)(2,1)} %bitcast.65, bf16[512,1024]{1,0:T(8,128)(2,1)} %param.31, bf16[512,1024]{1,0:T(8,128)(2,1)} %param.30, f32[512]{0:T(512)S(1)} %dynamic_slice.7, f32[8]{0:T(128)S(1)} %add_rsqrt_fusion.2, bf16[8,2048]{1,0:T(8,128)(2,1)S(1)} %all_gather.13, ...), kind=kOutput, calls=%fused_computation | convolution fusion | flops 31670272 | bytes 2845700 | tf_op jit(solution)/shard_map/dot_general | solution.py:70
  79.8 0.0 all-reduce.3.cloned.1.call-update
  79.9 0.0 reduce-scatter.6.cloned.1.call-start
  79.9 0.0 copy-done.14
  80.0 0.6 dynamic-slice
  81.2 31.1 %all-reduce.3.cloned.1.call-done = f32[8,2576]{1,0:T(8,128)} async-done(((f32[8,2576]{1,0:T(8,128)}), f32[8,2576]{1,0:T(8,128)}) %all-reduce.3.cloned.1.call-update) | async-done | bytes 82448
  112.3 0.9 dynamic-slice_convert_fusion
  113.4 0.1 reshape.69
  113.5 0.0 copy-done.13
  113.5 0.8 multiply_exponential_fusion
  114.3 0.1 broadcast_multiply_fusion
  114.4 1.6 multiply_add_fusion
  116.0 0.0 copy-start.1
  116.1 0.9 copy-done.1
  117.0 0.4 fusion.58
  117.4 0.1 multiply_add_fusion.1
  117.5 0.1 reshape.71
  117.6 0.1 reduce_sum.38
  117.7 0.1 broadcast_bitcast_fusion.1
  117.8 13.2 %all-gather = bf16[4,2,1024]{2,1,0:T(2,128)(2,1)S(1)} all-gather(bf16[1,2,1024]{2,1,0:T(2,128)(2,1)S(1)} %fusion.48), channel_id=1, replica_groups=mesh['dp'=4,'kv'=4,'tp'=2] {'kv'}, dimensions={0}, use_global_device_ids=true | all-gather | bytes 20480 | tf_op jit(solution)/shard_map/all_gather | solution.py:112
  131.1 2.1 %convolution_convert_fusion = bf16[8,512]{1,0:T(8,128)(2,1)} fusion(bf16[8,1024]{1,0:T(8,128)(2,1)S(1)} %reshape.73, bf16[1024,512]{1,0:T(8,128)(2,1)} %param.43), kind=kOutput, calls=%fused_computation.14 | convolution fusion | flops 8392704 | bytes 1073152 | tf_op jit(solution)/shard_map/dot_general | solution.py:111
  133.1 0.0 reduce-scatter.6.cloned.1.call-update
  133.2 0.0 reduce-scatter.8.cloned.1.call-start
  133.2 7.6 %reduce-scatter.6.cloned.1.call-done = bf16[8,256]{1,0:T(8,128)(2,1)} async-done(((bf16[8,512]{1,0:T(8,128)(2,1)}), bf16[8,256]{1,0:T(8,128)(2,1)}) %reduce-scatter.6.cloned.1.call-update) | async-done | bytes 4112 | tf_op jit(solution)/shard_map/reduce_scatter | solution.py:116
  140.8 0.7 add_convert_fusion.1
  141.5 14.3 %all_gather.15 = bf16[8,2048]{1,0:T(8,128)(2,1)S(1)} all-gather(bf16[8,256]{1,0:T(8,128)(2,1)S(1)} %add_convert_fusion.1), channel_id=1, replica_groups=mesh['dp'=4,'kv'=4,'tp'=2] {'kv','tp'}, dimensions={1}, use_global_device_ids=true | all-gather | bytes 36864 | tf_op jit(solution)/shard_map/all_gather | solution.py:16
  155.8 0.1 fusion.15
  156.0 2.7 %fusion.42 = f32[8,704]{1,0:T(8,128)S(1)} fusion(bf16[2048,704]{0,1:T(8,128)(2,1)} %param.45, bf16[8,2048]{1,0:T(8,128)(2,1)S(1)} %all_gather.15, f32[2048]{0:T(1024)S(1)} %copy-done.5, f32[8]{0:T(128)S(1)} %add_rsqrt_fusion.1), kind=kOutput, calls=%fused_computation.69 | convolution fusion | flops 23134208 | bytes 2947104 | tf_op jit(solution)/shard_map/dot_general | solution.py:18
  158.6 5.0 %fusion.10 = f32[8,2048]{1,0:T(8,128)} fusion(bf16[704,2048]{1,0:T(8,128)(2,1)} %param.47, bf16[2048,704]{0,1:T(8,128)(2,1)} %param.46, f32[8,704]{1,0:T(8,128)S(1)} %fusion.42, bf16[8,2048]{1,0:T(8,128)(2,1)S(1)} %all_gather.15, f32[2048]{0:T(1024)S(1)} %copy-done.5, f32[8]{0:T(128)S(1)} %add_rsqrt_fusion.1), kind=kOutput, calls=%fused_computation.12 | convolution fusion | flops 46236672 | bytes 5896224 | tf_op jit(solution)/shard_map/dot_general | solution.py:21
  163.6 0.0 reduce-scatter.8.cloned.1.call-update
  163.6 0.6 fusion.39
  164.2 0.6 fusion.28
  164.8 30.2 %reduce-scatter.8.cloned.1.call-done = f32[8,256]{1,0:T(8,128)} async-done(((f32[8,2048]{1,0:T(8,128)}), f32[8,256]{1,0:T(8,128)}) %reduce-scatter.8.cloned.1.call-update) | async-done | bytes 8208 | tf_op jit(solution)/shard_map/reduce_scatter | solution.py:22
  195.1 1.3 add_convert_fusion
  (36 shorter events, 0.3 us)
Async XLA Ops:
  7.2 19.0 %copy-start = (bf16[704,2048]{1,0:T(8,128)(2,1)S(1)}, bf16[704,2048]{1,0:T(8,128)(2,1)}, u32[]{:S(2)}) copy-start(bf16[704,2048]{1,0:T(8,128)(2,1)} %param.28) | copy-start | bytes 8650756
  7.2 18.9 %copy-start.4 = (f32[2048]{0:T(1024)S(1)}, f32[2048]{0:T(1024)}, u32[]{:S(2)}) copy-start(f32[2048]{0:T(1024)} %param.25) | copy-start | bytes 24580
  7.2 54.8 %reduce-scatter.4.cloned.1.call-start = ((), (), s32[]{:S(2)}) async-start(), calls=%async_computation.3 | async-start | bytes 73728 | tf_op jit(solution)/shard_map/reduce_scatter | solution.py:22
  26.1 4.3 %copy-start.2 = (bf16[512,2,256]{2,1,0:T(2,128)(2,1)S(1)}, bf16[512,2,256]{2,1,0:T(2,128)(2,1)}, u32[]{:S(2)}) copy-start(bf16[512,2,256]{2,1,0:T(2,128)(2,1)} %param.32) | copy-start | bytes 1572868
  26.1 5.2 %copy-start.7 = (bf16[512,16]{0,1:T(8,128)(2,1)S(1)}, bf16[512,16]{0,1:T(8,128)(2,1)}, u32[]{:S(2)}) copy-start(bf16[512,16]{0,1:T(8,128)(2,1)} %param.33) | copy-start | bytes 49156
  26.2 6.0 %copy-start.9 = (bf16[4,1024]{1,0:T(4,128)(2,1)S(1)}, bf16[4,1024]{1,0:T(4,128)(2,1)}, u32[]{:S(2)}) copy-start(bf16[4,1024]{1,0:T(4,128)(2,1)} %param.34) | copy-start | bytes 24580
  26.2 35.8 %copy-start.8 = (bf16[8,256]{1,0:T(8,128)(2,1)S(1)}, bf16[8,256]{1,0:T(8,128)(2,1)}, u32[]{:S(2)}) copy-start(bf16[8,256]{1,0:T(8,128)(2,1)} %param.24) | copy-start | bytes 12292
  30.3 82.0 %all-reduce.3.cloned.1.call-start = ((), (), s32[]{:S(2)}) async-start(), calls=%async_computation.6 | async-start | bytes 172032
  76.9 3.0 %copy-start.10 = (bf16[4,2,256]{2,1,0:T(2,128)(2,1)S(1)}, bf16[4,2,256]{2,1,0:T(2,128)(2,1)}, u32[]{:S(2)}) copy-start(bf16[4,2,256]{2,1,0:T(2,128)(2,1)} %param.35) | copy-start | bytes 12292
  76.9 3.0 %copy-start.14 = (f32[16]{0:T(128)S(1)}, f32[16]{0:T(128)}, u32[]{:S(2)}) copy-start(f32[16]{0:T(128)} %param.40) | copy-start | bytes 196
  76.9 3.1 %copy-start.15 = (u32[32]{0:T(128)S(1)}, u32[32]{0:T(128)}, u32[]{:S(2)}) copy-start(u32[32]{0:T(128)} %constant.47) | copy-start | bytes 388
  76.9 36.3 %copy-start.3 = (bf16[2,3,1024]{2,0,1:T(2,128)(2,1)S(1)}, bf16[2,3,1024]{2,0,1:T(2,128)(2,1)}, u32[]{:S(2)}) copy-start(bf16[2,3,1024]{2,0,1:T(2,128)(2,1)} %param.36) | copy-start | bytes 36868
  76.9 36.5 %copy-start.6 = (bf16[2,3,2,256]{3,2,1,0:T(2,128)(2,1)S(1)}, bf16[2,3,2,256]{3,2,1,0:T(2,128)(2,1)}, u32[]{:S(2)}) copy-start(bf16[2,3,2,256]{3,2,1,0:T(2,128)(2,1)} %param.37) | copy-start | bytes 18436
  77.0 36.6 %copy-start.13 = (f32[16]{0:T(128)S(1)}, f32[16]{0:T(128)}, u32[]{:S(2)}) copy-start(f32[16]{0:T(128)} %param.39) | copy-start | bytes 196
  79.8 37.5 %copy-start.12 = (f32[16]{0:T(128)S(1)}, f32[16]{0:T(128)}, u32[]{:S(2)}) copy-start(f32[16]{0:T(128)} %param.41) | copy-start | bytes 196
  79.8 37.9 %copy-start.11 = (f32[1024]{0:T(1024)S(1)}, f32[1024]{0:T(1024)}, u32[]{:S(2)}) copy-start(f32[1024]{0:T(1024)} %param.42) | copy-start | bytes 12292
  79.8 76.1 %copy-start.5 = (f32[2048]{0:T(1024)S(1)}, f32[2048]{0:T(1024)}, u32[]{:S(2)}) copy-start(f32[2048]{0:T(1024)} %param.44) | copy-start | bytes 24580
  79.9 60.9 %reduce-scatter.6.cloned.1.call-start = ((), (), s32[]{:S(2)}) async-start(), calls=%async_computation.4 | async-start | bytes 12288 | tf_op jit(solution)/shard_map/reduce_scatter | solution.py:116
  116.0 1.0 copy-start.1
  133.2 61.9 %reduce-scatter.8.cloned.1.call-start = ((), (), s32[]{:S(2)}) async-start(), calls=%async_computation.5 | async-start | bytes 73728 | tf_op jit(solution)/shard_map/reduce_scatter | solution.py:22
Sparse Core Ops, SparseCore 0:
  30.5 31.4 reduce-scatter.3
  80.0 32.3 all-reduce.2
  133.3 7.4 reduce-scatter.5
  163.7 31.2 reduce-scatter.7
where the time goes:
time: 203 us
  waiting for transfers between devices  98.8 us (49%)
  blocking collectives  57.7 us (28%)
  matrix products  19.8 us (10%)
  between operations  14.7 us (7%)
  other arithmetic  7.11 us (4%)
  local copies, waits for them, and re-layouts  4.65 us (2%)
    reduce_scatter x2, waiting for transfers between devices, half_mlp(): lax.psum_scatter(partial_sums, ('kv', 'tp'), scatter_dimension=1, tiled=T...  60 us
    unnamed x5, waiting for transfers between devices  31.2 us
    all_gather x2, blocking collectives, half_mlp(): gathered = lax.all_gather(columns, ('kv', 'tp'), axis=1, tiled=True)  30.4 us
    all_gather x1, blocking collectives, per_device(): gathered = lax.all_gather(after_first, ('kv', 'tp'), axis=1, tiled=True)  14.1 us
    all_gather x1, blocking collectives, per_device(): lax.all_gather(mixed, 'kv', axis=0, tiled=True)  13.2 us
    dot_general x2, matrix products, half_mlp(): jnp.dot(hidden, down_weight, preferred_element_type=jnp.float32)  9.13 us
    reduce_scatter x1, waiting for transfers between devices, per_device(): lax.psum_scatter(partial_out.astype(jnp.bfloat16), 'tp', scatter_dimensio...  7.61 us
    dot_general x2, matrix products, half_mlp(): gate_part = jnp.dot(normed, gate_weight, preferred_element_type=jnp.float32)  5.33 us
  transfers between devices with their start and end apart: 4, of which 4 were waited for; matrix products, arithmetic and copies ran while one was open for 2% of the time, Pallas kernels for 0%

commit v1 on v0

--- a/solution.py
+++ b/solution.py
@@ -1,6 +1,10 @@
+import functools
+
 import jax
 import jax.numpy as jnp
 from jax import lax
+from jax.experimental import pallas as pl
+from jax.experimental.pallas import tpu as pltpu
 from jax.sharding import PartitionSpec as P
 
 EPS = 1e-06
@@ -23,7 +27,7 @@
     return (columns.astype(jnp.float32) + 0.5 * summed).astype(jnp.bfloat16)
 
 
-def per_device(
+def plain_device(
     tokens,
     mlp1_gain,
     mlp1_gate,
@@ -121,6 +125,520 @@
     return (result, new_state, full_x[:, 1:], full_bc[:, 1:])
 
 
+MESH = pl.DeviceIdType.MESH
+F32 = jnp.float32
+BF16 = jnp.bfloat16
+TOKENS, SUM1, PROJ, EXTRA, FIRST, MIXED, OUT, SUM2 = range(8)
+PHASES = 8
+
+
+def dot32(left, right):
+    return jnp.dot(left, right, preferred_element_type=F32)
+
+
+def fused_kernel(
+    n_kv,
+    n_tp,
+    tokens,
+    gain1,
+    gate1,
+    up1,
+    down1,
+    gain_m,
+    proj_z,
+    proj_x,
+    proj_bc,
+    proj_dt,
+    conv_x,
+    conv_bc,
+    window_x,
+    window_bc,
+    state,
+    dt_bias,
+    log_rate,
+    skip_gain,
+    group_gain,
+    out_weight,
+    gain2,
+    gate2,
+    up2,
+    down2,
+    result,
+    step_x_out,
+    retain_out,
+    b_out,
+    x_new_out,
+    bc_new_out,
+    tok_v,
+    gain1_v,
+    gate1_v,
+    up1_v,
+    down1_v,
+    gain_m_v,
+    z_v,
+    x_v,
+    bc_v,
+    dt_v,
+    conv_x_v,
+    conv_bc_v,
+    window_x_v,
+    window_bc_v,
+    state_v,
+    bias_v,
+    log_v,
+    skip_v,
+    ggain_v,
+    out_v,
+    gain2_v,
+    gate2_v,
+    up2_v,
+    down2_v,
+    state_half,
+    tok_all,
+    sum1_send,
+    sum1_all,
+    proj_send,
+    proj_all,
+    extra_send,
+    extra_all,
+    first_all,
+    mixed_all,
+    out_all,
+    sum2_send,
+    sum2_all,
+    local_sem,
+    send_sem,
+    recv_sem,
+):
+    n = n_kv * n_tp
+    kv, tp = lax.axis_index("kv"), lax.axis_index("tp")
+    me = kv * n_tp + tp
+    rows, cols = tok_v.shape
+    width = cols * n
+    kv_cols = cols * n_tp
+    used = [0]
+
+    def load(source, target):
+        copy = pltpu.make_async_copy(source, target, local_sem.at[used[0]])
+        used[0] += 1
+        copy.start()
+        return copy
+
+    chunk = cols
+    tok_copies = [load(tokens, tok_v), load(gain1, gain1_v)]
+    gu1 = []
+    for i in range(n):
+        part = pl.ds(i * chunk, chunk)
+        gu1.append((load(gate1.at[part], gate1_v.at[part]), load(up1.at[part], up1_v.at[part])))
+    down1_copy = load(down1, down1_v)
+    proj_copies = [
+        load(gain_m, gain_m_v),
+        load(proj_z, z_v),
+        load(proj_x, x_v),
+        load(proj_bc, bc_v),
+        load(proj_dt, dt_v),
+    ]
+    ssm_copies = [
+        load(conv_x, conv_x_v),
+        load(conv_bc, conv_bc_v),
+        load(window_x, window_x_v),
+        load(window_bc, window_bc_v),
+        load(dt_bias, bias_v),
+        load(log_rate, log_v),
+        load(skip_gain, skip_v),
+        load(group_gain, ggain_v),
+        load(state, state_v),
+    ]
+    out_copy = load(out_weight, out_v)
+    gain2_copy = load(gain2, gain2_v)
+    gu2 = [load(gate2, gate2_v), load(up2, up2_v)]
+    down2_copy = load(down2, down2_v)
+
+    def peer_of(offset):
+        peer = lax.rem(me + offset, n)
+        return peer, lax.div(peer, n_tp), lax.rem(peer, n_tp)
+
+    barrier = pltpu.get_barrier_semaphore()
+    for offset in range(1, n):
+        _, peer_kv, peer_tp = peer_of(offset)
+        pl.semaphore_signal(
+            barrier, inc=1, device_id={"kv": peer_kv, "tp": peer_tp}, device_id_type=MESH
+        )
+    pl.semaphore_wait(barrier, n - 1)
+
+    sends = []
+
+    def send(source, target, phase, slot, source_slot, to_kv, to_tp):
+        copy = pltpu.make_async_remote_copy(
+            src_ref=source,
+            dst_ref=target,
+            send_sem=send_sem.at[phase, slot],
+            recv_sem=recv_sem.at[phase, source_slot],
+            device_id={"kv": to_kv, "tp": to_tp},
+            device_id_type=MESH,
+        )
+        copy.start()
+        sends.append(copy)
+
+    def arrive(target, phase, source_slot):
+        pltpu.make_async_remote_copy(
+            src_ref=target,
+            dst_ref=target,
+            send_sem=send_sem.at[phase, 0],
+            recv_sem=recv_sem.at[phase, source_slot],
+            device_id={"kv": kv, "tp": tp},
+            device_id_type=MESH,
+        ).wait_recv()
+
+    for copy in tok_copies:
+        copy.wait()
+    for offset in range(1, n):
+        _, peer_kv, peer_tp = peer_of(offset)
+        send(tok_v, tok_all.at[me], TOKENS, offset, me, peer_kv, peer_tp)
+    tok_all[me] = tok_v[...]
+    for offset in range(1, n):
+        peer, _, _ = peer_of(offset)
+        arrive(tok_all.at[peer], TOKENS, peer)
+
+    def hidden_of(parts, gain_ref, gate_ref, up_ref, ready):
+        squares = sum(jnp.sum(v * v, axis=1, keepdims=True) for v in parts)
+        factor = lax.rsqrt(squares / width + EPS)
+        gate_part = up_part = None
+        for i, v in enumerate(parts):
+            piece = v.shape[1]
+            part = pl.ds(i * piece, piece)
+            normed = (v * factor * gain_ref[:, part]).astype(BF16)
+            ready(i)
+            a, b = dot32(normed, gate_ref[part, :]), dot32(normed, up_ref[part, :])
+            gate_part = a if i == 0 else gate_part + a
+            up_part = b if i == 0 else up_part + b
+        return (jax.nn.silu(gate_part) * up_part).astype(BF16)
+
+    def ready1(i):
+        for copy in gu1[i]:
+            copy.wait()
+
+    hidden1 = hidden_of(
+        [tok_all[i].astype(F32) for i in range(n)], gain1_v, gate1_v, up1_v, ready1
+    )
+    down1_copy.wait()
+    for step in range(1, n_kv + 1):
+        to_kv = lax.rem(kv + step, n_kv)
+        part = pl.ds(pl.multiple_of(to_kv * kv_cols, 128), kv_cols)
+        partial_sum = dot32(hidden1, down1_v[:, part]).astype(BF16)
+        if step < n_kv:
+            sum1_send[step] = partial_sum
+            for other in range(n_tp):
+                to_tp = lax.rem(tp + other, n_tp)
+                send(
+                    sum1_send.at[step],
+                    sum1_all.at[me],
+                    SUM1,
+                    step * n_tp + other,
+                    me,
+                    to_kv,
+                    to_tp,
+                )
+        else:
+            sum1_all[me] = partial_sum
+            sum1_send[0] = partial_sum
+            for other in range(1, n_tp):
+                to_tp = lax.rem(tp + other, n_tp)
+                send(sum1_send.at[0], sum1_all.at[me], SUM1, other, me, kv, to_tp)
+
+    for copy in ssm_copies:
+        copy.wait()
+    seqs = window_x_v.shape[0]
+    state_size = state_v.shape[2]
+    heads = dt_v.shape[1]
+    inner = z_v.shape[1]
+    group_width = bc_v.shape[1] // 2
+    groups = group_width // state_size
+    head_dim = inner // heads
+    group_inner = inner // groups
+    taps = conv_x_v.shape[0]
+    conv_xf = conv_x_v[...].astype(F32)
+    past_x = jnp.concatenate(
+        [
+            jnp.sum(window_x_v[s].astype(F32) * conv_xf[: taps - 1], axis=0, keepdims=True)
+            for s in range(seqs)
+        ],
+        axis=0,
+    )
+    conv_bcf = conv_bc_v[...].astype(F32)
+    past_bc = jnp.concatenate(
+        [
+            jnp.sum(window_bc_v[s].astype(F32) * conv_bcf[: taps - 1], axis=0, keepdims=True)
+            for s in range(seqs)
+        ],
+        axis=0,
+    )
+    state_half[...] = state_v[...].astype(BF16)
+    lanes = lax.broadcasted_iota(jnp.int32, (heads, inner), 1)
+    owner = lax.broadcasted_iota(jnp.int32, (heads, inner), 0)
+    low = owner * head_dim
+    spread = jnp.where((lanes >= low) & (lanes < low + head_dim), 1.0, 0.0).astype(F32)
+
+    def expand(values):
+        return jnp.dot(
+            values, spread, preferred_element_type=F32, precision=lax.Precision.HIGHEST
+        )
+
+    skip = expand(jnp.broadcast_to(skip_v[...], (8, heads)))[:seqs]
+    for copy in proj_copies:
+        copy.wait()
+
+    for offset in range(1, n):
+        peer, _, _ = peer_of(offset)
+        arrive(sum1_all.at[peer], SUM1, peer)
+    summed = sum1_all[0].astype(F32)
+    for i in range(1, n):
+        summed = summed + sum1_all[i].astype(F32)
+    base = jnp.concatenate([tok_all[kv * n_tp + t].astype(F32) for t in range(n_tp)], axis=1)
+    after = (base + 0.5 * summed).astype(BF16)
+    first_all[kv] = after
+    after32 = after.astype(F32)
+    squares = jnp.sum(after32 * after32, axis=1, keepdims=True)
+    gain_part = gain_m_v[:, pl.ds(pl.multiple_of(kv * kv_cols, 128), kv_cols)]
+    scaled = (after32 * gain_part).astype(BF16)
+    own_rates = dot32(scaled, dt_v[...])
+    for k in range(n_kv):
+        rows_k = slice(k * seqs, (k + 1) * seqs)
+        extra_send[k] = jnp.broadcast_to(squares[rows_k], (seqs, extra_send.shape[2]))
+        extra_send[k, :, :heads] = own_rates[rows_k]
+    for place, weight in ((0, z_v), (inner, x_v), (2 * inner, bc_v)):
+        piece = dot32(scaled, weight[...])
+        for k in range(n_kv):
+            proj_send[k, :, pl.ds(place, weight.shape[1])] = piece[
+                k * seqs : (k + 1) * seqs
+            ].astype(BF16)
+    proj_all[kv] = proj_send[kv]
+    extra_all[kv] = extra_send[kv]
+    for step in range(1, n_kv):
+        to_kv = lax.rem(kv + step, n_kv)
+        send(proj_send.at[to_kv], proj_all.at[kv], PROJ, step, kv, to_kv, tp)
+        send(extra_send.at[to_kv], extra_all.at[kv], EXTRA, step, kv, to_kv, tp)
+    for step in range(1, n_kv):
+        to_kv = lax.rem(kv + step, n_kv)
+        send(first_all.at[kv], first_all.at[kv], FIRST, step, kv, to_kv, tp)
+
+    for step in range(1, n_kv):
+        from_kv = lax.rem(kv + step, n_kv)
+        arrive(extra_all.at[from_kv], EXTRA, from_kv)
+        arrive(proj_all.at[from_kv], PROJ, from_kv)
+    extra = extra_all[0]
+    projected = proj_all[0].astype(F32)
+    for k in range(1, n_kv):
+        extra = extra + extra_all[k]
+        projected = projected + proj_all[k].astype(F32)
+    factor = lax.rsqrt(extra[:, heads : heads + 1] / width + EPS)
+    projected = projected * factor
+    step_size = extra[:, :heads] * factor + bias_v[...]
+    step_size = jnp.maximum(step_size, 0.0) + jnp.log1p(jnp.exp(-jnp.abs(step_size)))
+    retain = jnp.exp(-step_size * jnp.exp(log_v[...]))
+    gate_z = projected[:, :inner].astype(BF16).astype(F32)
+    x_new = projected[:, inner : 2 * inner].astype(BF16)
+    bc_new = projected[:, 2 * inner :].astype(BF16)
+    mixed_x = jax.nn.silu(past_x + conv_xf[taps - 1 :] * x_new.astype(F32))
+    mixed_bc = jax.nn.silu(past_bc + conv_bcf[taps - 1 :] * bc_new.astype(F32))
+    step_x = expand(step_size) * mixed_x
+    retained = expand(retain)
+    pieces = []
+    which = lax.broadcasted_iota(jnp.int32, (seqs, group_inner), 0)
+    for g in range(groups):
+        b = mixed_bc[:, g * state_size : (g + 1) * state_size]
+        c = mixed_bc[:, group_width + g * state_size : group_width + (g + 1) * state_size]
+        span = slice(g * group_inner, (g + 1) * group_inner)
+        old = None
+        for s in range(seqs):
+            read = lax.dot_general(
+                c.astype(BF16),
+                state_half[s, g * group_inner : (g + 1) * group_inner, :],
+                (((1,), (1,)), ((), ())),
+                preferred_element_type=F32,
+            )
+            old = read if s == 0 else jnp.where(which == s, read, old)
+        match = jnp.sum(b * c, axis=1, keepdims=True)
+        readout = retained[:, span] * old + step_x[:, span] * match + skip[:, span] * mixed_x[:, span]
+        z = gate_z[:, span]
+        gated = readout * jax.nn.silu(z)
+        gated = gated * lax.rsqrt(jnp.mean(gated * gated, axis=1, keepdims=True) + EPS)
+        pieces.append((gated * ggain_v[:, span]).astype(BF16))
+    mixed_all[kv] = jnp.concatenate(pieces, axis=1)
+    for step in range(1, n_kv):
+        to_kv = lax.rem(kv + step, n_kv)
+        send(mixed_all.at[kv], mixed_all.at[kv], MIXED, step, kv, to_kv, tp)
+    step_x_out[...] = step_x
+    retain_out[...] = retain
+    b_out[...] = mixed_bc[:, :group_width]
+    x_new_out[...] = x_new
+    bc_new_out[...] = bc_new
+    out_copy.wait()
+    for step in range(1, n_kv):
+        from_kv = lax.rem(kv + step, n_kv)
+        arrive(mixed_all.at[from_kv], MIXED, from_kv)
+    mixed = jnp.concatenate([mixed_all[k].astype(F32) for k in range(n_kv)], axis=0)
+    out_all[me] = dot32(mixed.astype(BF16), out_v[...]).astype(BF16)
+    for offset in range(1, n):
+        _, peer_kv, peer_tp = peer_of(offset)
+        send(out_all.at[me], out_all.at[me], OUT, offset, me, peer_kv, peer_tp)
+
+    gain2_copy.wait()
+    for copy in gu2:
+        copy.wait()
+    down2_copy.wait()
+    for step in range(1, n_kv):
+        from_kv = lax.rem(kv + step, n_kv)
+        arrive(first_all.at[from_kv], FIRST, from_kv)
+    for offset in range(1, n):
+        peer, _, _ = peer_of(offset)
+        arrive(out_all.at[peer], OUT, peer)
+
+    def after_of(k):
+        total = out_all[k * n_tp].astype(F32)
+        for t in range(1, n_tp):
+            total = total + out_all[k * n_tp + t].astype(F32)
+        return (first_all[k].astype(F32) + total).astype(BF16).astype(F32)
+
+    hidden2 = hidden_of(
+        [after_of(k) for k in range(n_kv)], gain2_v, gate2_v, up2_v, lambda i: None
+    )
+    for offset in range(1, n + 1):
+        peer, peer_kv, peer_tp = peer_of(offset)
+        part = pl.ds(pl.multiple_of(peer * cols, 128), cols)
+        partial_sum = dot32(hidden2, down2_v[:, part]).astype(BF16)
+        if offset < n:
+            sum2_send[offset] = partial_sum
+            send(sum2_send.at[offset], sum2_all.at[me], SUM2, offset, me, peer_kv, peer_tp)
+        else:
+            sum2_all[me] = partial_sum
+    own = after_of(kv)
+    mine = own[:, :cols]
+    for t in range(1, n_tp):
+        mine = jnp.where(tp == t, own[:, t * cols : (t + 1) * cols], mine)
+    for offset in range(1, n):
+        peer, _, _ = peer_of(offset)
+        arrive(sum2_all.at[peer], SUM2, peer)
+    summed = sum2_all[0].astype(F32)
+    for i in range(1, n):
+        summed = summed + sum2_all[i].astype(F32)
+    result[...] = (mine + 0.5 * summed).astype(BF16)
+    for copy in sends:
+        copy.wait_send()
+
+
+def per_device(n_kv, n_tp, *args):
+    (
+        tokens,
+        mlp1_gain,
+        mlp1_gate,
+        mlp1_up,
+        mlp1_down,
+        mixer_gain,
+        proj_z,
+        proj_x,
+        proj_bc,
+        proj_dt,
+        conv_x,
+        conv_bc,
+        window_x,
+        window_bc,
+        ssm_state,
+        dt_bias,
+        log_rate,
+        skip_gain,
+        group_gain,
+        out_weight,
+        mlp2_gain,
+        mlp2_gate,
+        mlp2_up,
+        mlp2_down,
+    ) = args
+    rows, cols = tokens.shape
+    if cols % 128 or n_kv * n_tp > 16 or rows % 8:
+        return plain_device(*args)
+    n = n_kv * n_tp
+    kv_cols = cols * n_tp
+    seqs, heads = window_x.shape[0], proj_dt.shape[1]
+    inner, group_width = proj_z.shape[1], proj_bc.shape[2]
+    state_size = ssm_state.shape[3]
+    groups = group_width // state_size
+    taps = conv_x.shape[0]
+    operands = (
+        tokens,
+        mlp1_gain[None],
+        mlp1_gate,
+        mlp1_up,
+        mlp1_down,
+        mixer_gain[None],
+        proj_z,
+        proj_x,
+        proj_bc.reshape(proj_bc.shape[0], 2 * group_width),
+        proj_dt,
+        conv_x,
+        conv_bc.reshape(taps, 2 * group_width),
+        window_x,
+        window_bc.reshape(seqs, taps - 1, 2 * group_width),
+        ssm_state.reshape(seqs, inner, state_size),
+        dt_bias[None],
+        log_rate[None],
+        skip_gain[None],
+        group_gain[None],
+        out_weight,
+        mlp2_gain[None],
+        mlp2_gate,
+        mlp2_up,
+        mlp2_down,
+    )
+    vmem = [pltpu.VMEM(a.shape, a.dtype) for a in operands]
+    scratch = vmem + [
+        pltpu.VMEM((seqs, inner, state_size), BF16),
+        pltpu.VMEM((n, rows, cols), BF16),
+        pltpu.VMEM((n_kv, rows, kv_cols), BF16),
+        pltpu.VMEM((n, rows, kv_cols), BF16),
+        pltpu.VMEM((n_kv, seqs, 2 * inner + 2 * group_width), BF16),
+        pltpu.VMEM((n_kv, seqs, 2 * inner + 2 * group_width), BF16),
+        pltpu.VMEM((n_kv, seqs, 128), F32),
+        pltpu.VMEM((n_kv, seqs, 128), F32),
+        pltpu.VMEM((n_kv, rows, kv_cols), BF16),
+        pltpu.VMEM((n_kv, seqs, inner), BF16),
+        pltpu.VMEM((n, rows, kv_cols), BF16),
+        pltpu.VMEM((n, rows, cols), BF16),
+        pltpu.VMEM((n, rows, cols), BF16),
+        pltpu.SemaphoreType.DMA((2 * n + 40,)),
+        pltpu.SemaphoreType.DMA((PHASES, n)),
+        pltpu.SemaphoreType.DMA((PHASES, n)),
+    ]
+    shapes = (
+        jax.ShapeDtypeStruct((rows, cols), BF16),
+        jax.ShapeDtypeStruct((seqs, inner), F32),
+        jax.ShapeDtypeStruct((seqs, heads), F32),
+        jax.ShapeDtypeStruct((seqs, group_width), F32),
+        jax.ShapeDtypeStruct((seqs, inner), BF16),
+        jax.ShapeDtypeStruct((seqs, 2 * group_width), BF16),
+    )
+    result, step_x, retain, keys_b, x_new, bc_new = pl.pallas_call(
+        functools.partial(fused_kernel, n_kv, n_tp),
+        out_shape=shapes,
+        in_specs=[pl.BlockSpec(memory_space=pl.ANY)] * len(operands),
+        out_specs=[pl.BlockSpec(memory_space=pltpu.VMEM)] * len(shapes),
+        scratch_shapes=scratch,
+        compiler_params=pltpu.CompilerParams(
+            collective_id=0, has_side_effects=True, vmem_limit_bytes=60 * 1024 * 1024
+        ),
+    )(*operands)
+    keys_b = jnp.repeat(keys_b.reshape(seqs, groups, state_size), heads // groups, axis=1)
+    new_state = (
+        retain[:, :, None, None] * ssm_state
+        + step_x.reshape(seqs, heads, inner // heads)[:, :, :, None] * keys_b[:, :, None, :]
+    )
+    new_x = jnp.concatenate([window_x[:, 1:], x_new[:, None]], axis=1)
+    new_bc = jnp.concatenate(
+        [window_bc[:, 1:], bc_new.reshape(seqs, 1, 2, group_width)], axis=1
+    )
+    return (result, new_state, new_x, new_bc)
+
+
 def solution(mesh):
     placed = (
         P("dp", ("kv", "tp")),
@@ -149,7 +667,7 @@
         P(("kv", "tp"), None),
     )
     return jax.shard_map(
-        per_device,
+        functools.partial(per_device, mesh.shape["kv"], mesh.shape["tp"]),
         mesh=mesh,
         in_specs=placed,
         out_specs=(

time: 203 us -> 60.5 us (0.30)
  waiting for transfers between devices: 98.8 us -> 0 us
  blocking collectives: 57.7 us -> 0 us
  Pallas kernels: 0 us -> 33.5 us
  matrix products: 19.8 us -> 0 us
  local copies, waits for them, and re-layouts: 4.65 us -> 22.1 us
  between operations: 14.7 us -> 0.69 us
  other arithmetic: 7.11 us -> 3.87 us
    reduce_scatter x3 -> x0, waiting for transfers between devices: 67.6 us -> none  [the longest x2 60 us: half_mlp(): lax.psum_scatter(partial_sums, ('kv', 'tp'), scatter_dimension=1, tiled=T...]
    all_gather x4 -> x0, blocking collectives: 57.7 us -> none  [the longest x2 30.4 us: half_mlp(): gathered = lax.all_gather(columns, ('kv', 'tp'), axis=1, tiled=True)]
    pallas_call x0 -> x1, Pallas kernels: none -> 33.5 us  [per_device(): pl.pallas_call(functools.partial(fused_kernel, n_kv, n_tp), out_shape=sha...]
    unnamed x5 -> x0, waiting for transfers between devices: 31.2 us -> none
    dot_general x7 -> x0, matrix products: 19.8 us -> none  [the longest x2 9.13 us: half_mlp(): jnp.dot(hidden, down_weight, preferred_element_type=jnp.float32)]
    unnamed x38 -> x25, local copies, waits for them, and re-layouts: 2.74 us -> 19.4 us
    convert_element_type x3 -> x0, other arithmetic: 2.67 us -> none  [the longest x2 1.99 us: half_mlp(): return (columns.astype(jnp.float32) + 0.5 * summed).astype(jnp.bfloat16)]
  transfers between devices with their start and end apart: 4 -> 0, of which waited for: 4 -> 0; matrix products, arithmetic and copies ran while one was open for 2% -> 0% of each run, Pallas kernels for 0% -> 0%
where the time goes in v1:
time: 60.5 us; the launch traced here: 60.1 us
  Pallas kernels  33.5 us (55%)
  local copies, waits for them, and re-layouts  22.1 us (37%)
  other arithmetic  3.87 us (6%)
  between operations  0.69 us (1%)
    pallas_call x1, Pallas kernels, per_device(): pl.pallas_call(functools.partial(fused_kernel, n_kv, n_tp), out_shape=sha...  33.5 us
    unnamed x25, local copies, waits for them, and re-layouts  19.4 us
    add x1, other arithmetic, per_device(): retain[:, :, None, None] * ssm_state  1.98 us
    concatenate x1, other arithmetic, per_device(): new_x = jnp.concatenate([window_x[:, 1:], x_new[:, None]], axis=1)  1.29 us

profile of v1, /device:TPU:0, one launch (start us, length us, event | category | flops | bytes accessed | tf_op | source)
XLA Modules:
  0.0 60.1 jit_solution(8670941184072308859)
XLA Ops:
  0.6 0.0 copy-start.1
  0.6 4.7 %copy.36.gate1 = bf16[2048,704]{1,0:T(8,128)(2,1)} copy(bf16[2048,704]{0,1:T(8,128)(2,1)} %param.26) | data formatting | bytes 5767168 | tf_op args[2]
  5.4 0.0 copy-done.1
  5.4 2.8 %copy.37.up1 = bf16[2048,704]{1,0:T(8,128)(2,1)} copy(bf16[2048,704]{0,1:T(8,128)(2,1)S(1)} %copy-done.1) | data formatting | bytes 5767168 | tf_op args[3]
  8.2 0.0 copy-start.2
  8.2 4.8 %copy.41.gate2 = bf16[2048,704]{1,0:T(8,128)(2,1)} copy(bf16[2048,704]{0,1:T(8,128)(2,1)} %param.45) | data formatting | bytes 5767168 | tf_op args[21]
  13.0 0.0 copy-done.2
  13.0 0.0 copy-start.3
  13.0 0.0 copy-start.6
  13.1 0.0 copy-start.4
  13.1 0.0 copy-start.5
  13.1 0.0 copy-start.7
  13.1 2.8 %copy.42.up2 = bf16[2048,704]{1,0:T(8,128)(2,1)} copy(bf16[2048,704]{0,1:T(8,128)(2,1)S(1)} %copy-done.2) | data formatting | bytes 5767168 | tf_op args[22]
  15.9 0.0 copy-done.3
  15.9 0.9 %copy.45 = bf16[64,8,2,256]{3,1,2,0:T(8,128)(2,1)} copy(bf16[64,8,2,256]{3,2,1,0:T(2,128)(2,1)S(1)} %bitcast.18) | data formatting | bytes 1048576
  16.8 0.0 copy-done.6
  16.8 0.8 %copy.38.proj_dt = bf16[512,16]{1,0:T(8,128)(2,1)} copy(bf16[512,16]{0,1:T(8,128)(2,1)S(1)} %copy-done.6) | data formatting | bytes 32768 | tf_op args[9]
  17.5 0.0 copy-done.4
  17.5 0.6 %copy.39.window_x = bf16[2,3,1024]{2,1,0:T(4,128)(2,1)} copy(bf16[2,3,1024]{2,0,1:T(2,128)(2,1)S(1)} %copy-done.4) | data formatting | bytes 24576 | tf_op args[12]
  18.2 0.0 copy-done.5
  18.2 0.6 %reshape.35.window_bc = bf16[2,3,512]{2,1,0:T(4,128)(2,1)} reshape(bf16[2,3,2,256]{3,2,1,0:T(2,128)(2,1)S(1)} %copy-done.5) | data formatting | bytes 12288 | tf_op jit(solution)/shard_map/reshape | solution.py:581
  18.8 0.0 copy-done.7
  18.8 0.6 copy.46
  19.4 0.0 copy-start
  19.4 0.0 slice-start
  19.4 0.0 slice-start.1
  19.4 33.5 %shard_map.255 = (bf16[8,256]{1,0:T(8,128)(2,1)}, f32[2,1024]{1,0:T(2,128)}, f32[2,16]{1,0:T(2,128)}, f32[2,256]{1,0:T(2,128)}, bf16[2,1024]{1,0:T(2,128)(2,1)}, /*index=5*/bf16[2,512]{1,0:T(2,128)(2,1)}) custom-call(bf16[8,256]{1,0:T(8,128)(2,1)} %tokens.1, f32[1,2048]{1,0:T(1,128)} %bitcast.20, bf16[2048,704]{1,0:T(8,128)(2,1)} %copy.36.gate1, ...), custom_call_target="tpu_custom_call" | custom-call | tf_op jit(solution)/shard_map/pallas_call | solution.py:620
  52.9 0.7 %reshape.33 = f32[2,2,128]{2,1,0:T(2,128)S(1)} reshape(f32[2,256]{1,0:T(2,128)} %get-tuple-element.13) | data formatting | bytes 4096 | tf_op jit(solution)/shard_map/reshape | solution.py:630
  53.6 0.8 %mul.27 = f32[2,16,64]{2,1,0:T(8,128)S(1)} reshape(f32[2,1024]{1,0:T(2,128)} %get-tuple-element.12) | data formatting | bytes 16384 | tf_op jit(solution)/shard_map/mul | solution.py:633
  54.3 0.0 copy-done
  54.4 2.0 %multiply_add_fusion = f32[2,16,64,128]{3,2,1,0:T(8,128)} fusion(f32[2,16,64,128]{3,2,1,0:T(8,128)S(1)} %copy-done, f32[2,16,128]{2,1,0:T(8,128)S(1)} %broadcast_bitcast_fusion, f32[2,16,64]{2,1,0:T(8,128)S(1)} %mul.27, f32[2,16]{1,0:T(2,128)} %get-tuple-element.11), kind=kLoop, calls=%fused_computation | loop fusion | flops 786432 | bytes 2121856 | tf_op jit(solution)/shard_map/add | solution.py:632
  56.3 0.0 slice-done
  56.3 1.3 %pad_maximum_fusion = bf16[2,3,1024]{2,0,1:T(2,128)(2,1)} fusion(bf16[2,1,1024]{2,0,1:T(2,128)(2,1)} %bitcast.25, bf16[2,2,1024]{2,0,1:T(2,128)(2,1)S(1)} %slice-done), kind=kLoop, calls=%fused_computation.1 | loop fusion | flops 6144 | bytes 24576 | tf_op jit(solution)/shard_map/concatenate | solution.py:635
  57.6 0.6 %reshape.34 = bf16[2,1,2,256]{3,2,0,1:T(2,128)(2,1)S(1)} reshape(bf16[2,512]{1,0:T(2,128)(2,1)} %get-tuple-element.15) | data formatting | bytes 4096 | tf_op jit(solution)/shard_map/reshape | solution.py:637
  58.3 0.0 slice-done.1
  58.3 0.6 %pad_maximum_fusion.1 = bf16[2,3,2,256]{3,2,1,0:T(2,128)(2,1)} fusion(bf16[2,1,2,256]{3,2,1,0:T(2,128)(2,1)S(1)} %bitcast.23, bf16[2,2,2,256]{3,2,1,0:T(2,128)(2,1)S(1)} %slice-done.1), kind=kLoop, calls=%fused_computation.3 | loop fusion | flops 3072 | bytes 12288 | tf_op jit(solution)/shard_map/concatenate | solution.py:636
  58.9 1.3 %copy.48 = bf16[8,256]{1,0:T(8,128)(2,1)} copy(bf16[8,256]{1,0:T(8,128)(2,1)} %get-tuple-element.20) | data formatting | bytes 8192
  (1 shorter events, 0.0 us)
Async XLA Ops:
  0.6 4.8 %copy-start.1 = (bf16[2048,704]{0,1:T(8,128)(2,1)S(1)}, bf16[2048,704]{0,1:T(8,128)(2,1)}, u32[]{:S(2)}) copy-start(bf16[2048,704]{0,1:T(8,128)(2,1)} %param.27) | copy-start | bytes 8650756
  8.2 4.9 %copy-start.2 = (bf16[2048,704]{0,1:T(8,128)(2,1)S(1)}, bf16[2048,704]{0,1:T(8,128)(2,1)}, u32[]{:S(2)}) copy-start(bf16[2048,704]{0,1:T(8,128)(2,1)} %param.46) | copy-start | bytes 8650756
  13.0 2.8 %copy-start.3 = (bf16[512,2,256]{2,1,0:T(2,128)(2,1)S(1)}, bf16[512,2,256]{2,1,0:T(2,128)(2,1)}, u32[]{:S(2)}) copy-start(bf16[512,2,256]{2,1,0:T(2,128)(2,1)} %param.32) | copy-start | bytes 1572868
  13.0 3.7 %copy-start.6 = (bf16[512,16]{0,1:T(8,128)(2,1)S(1)}, bf16[512,16]{0,1:T(8,128)(2,1)}, u32[]{:S(2)}) copy-start(bf16[512,16]{0,1:T(8,128)(2,1)} %param.33) | copy-start | bytes 49156
  13.1 4.5 %copy-start.4 = (bf16[2,3,1024]{2,0,1:T(2,128)(2,1)S(1)}, bf16[2,3,1024]{2,0,1:T(2,128)(2,1)}, u32[]{:S(2)}) copy-start(bf16[2,3,1024]{2,0,1:T(2,128)(2,1)} %param.36) | copy-start | bytes 36868
  13.1 5.1 %copy-start.5 = (bf16[2,3,2,256]{3,2,1,0:T(2,128)(2,1)S(1)}, bf16[2,3,2,256]{3,2,1,0:T(2,128)(2,1)}, u32[]{:S(2)}) copy-start(bf16[2,3,2,256]{3,2,1,0:T(2,128)(2,1)} %param.37) | copy-start | bytes 18436
  13.1 5.7 %copy-start.7 = (bf16[4,2,256]{2,1,0:T(2,128)(2,1)S(1)}, bf16[4,2,256]{2,1,0:T(2,128)(2,1)}, u32[]{:S(2)}) copy-start(bf16[4,2,256]{2,1,0:T(2,128)(2,1)} %param.35) | copy-start | bytes 12292
  19.4 35.0 %copy-start = (f32[2,16,64,128]{3,2,1,0:T(8,128)S(1)}, f32[2,16,64,128]{3,2,1,0:T(8,128)}, u32[]{:S(2)}) copy-start(f32[2,16,64,128]{3,2,1,0:T(8,128)} %param.38) | copy-start | bytes 3145732
  19.4 37.0 %slice-start = ((bf16[2,3,1024]{2,0,1:T(2,128)(2,1)}), bf16[2,2,1024]{2,0,1:T(2,128)(2,1)S(1)}, s32[]{:S(2)}) async-start(bf16[2,3,1024]{2,0,1:T(2,128)(2,1)} %param.36), calls=%async_computation | async-start | bytes 16384 | tf_op jit(solution)/shard_map/slice | solution.py:635
  19.4 38.9 %slice-start.1 = ((bf16[2,3,2,256]{3,2,1,0:T(2,128)(2,1)}), bf16[2,2,2,256]{3,2,1,0:T(2,128)(2,1)S(1)}, s32[]{:S(2)}) async-start(bf16[2,3,2,256]{3,2,1,0:T(2,128)(2,1)} %param.37), calls=%async_computation.1 | async-start | bytes 8192 | tf_op jit(solution)/shard_map/slice | solution.py:637

commit v2 on v1

--- a/solution.py
+++ b/solution.py
@@ -136,6 +136,10 @@
     return jnp.dot(left, right, preferred_element_type=F32)
 
 
+def dot32_rows(left, right):
+    return lax.dot_general(left, right, (((1,), (1,)), ((), ())), preferred_element_type=F32)
+
+
 def fused_kernel(
     n_kv,
     n_tp,
@@ -167,8 +171,8 @@
     step_x_out,
     retain_out,
     b_out,
-    x_new_out,
-    bc_new_out,
+    new_x_out,
+    new_bc_out,
     tok_v,
     gain1_v,
     gate1_v,
@@ -194,6 +198,7 @@
     up2_v,
     down2_v,
     state_half,
+    bc_halves,
     tok_all,
     sum1_send,
     sum1_all,
@@ -229,7 +234,9 @@
     gu1 = []
     for i in range(n):
         part = pl.ds(i * chunk, chunk)
-        gu1.append((load(gate1.at[part], gate1_v.at[part]), load(up1.at[part], up1_v.at[part])))
+        gu1.append(
+            (load(gate1.at[:, part], gate1_v.at[:, part]), load(up1.at[:, part], up1_v.at[:, part]))
+        )
     down1_copy = load(down1, down1_v)
     proj_copies = [
         load(gain_m, gain_m_v),
@@ -309,7 +316,7 @@
             part = pl.ds(i * piece, piece)
             normed = (v * factor * gain_ref[:, part]).astype(BF16)
             ready(i)
-            a, b = dot32(normed, gate_ref[part, :]), dot32(normed, up_ref[part, :])
+            a, b = dot32_rows(normed, gate_ref[:, part]), dot32_rows(normed, up_ref[:, part])
             gate_part = a if i == 0 else gate_part + a
             up_part = b if i == 0 else up_part + b
         return (jax.nn.silu(gate_part) * up_part).astype(BF16)
@@ -348,31 +355,33 @@
 
     for copy in ssm_copies:
         copy.wait()
-    seqs = window_x_v.shape[0]
+    seqs = window_x_v.shape[1]
     state_size = state_v.shape[2]
-    heads = dt_v.shape[1]
+    heads = dt_v.shape[0]
     inner = z_v.shape[1]
-    group_width = bc_v.shape[1] // 2
+    group_width = bc_v.shape[2]
     groups = group_width // state_size
     head_dim = inner // heads
     group_inner = inner // groups
     taps = conv_x_v.shape[0]
     conv_xf = conv_x_v[...].astype(F32)
-    past_x = jnp.concatenate(
-        [
-            jnp.sum(window_x_v[s].astype(F32) * conv_xf[: taps - 1], axis=0, keepdims=True)
-            for s in range(seqs)
-        ],
-        axis=0,
-    )
-    conv_bcf = conv_bc_v[...].astype(F32)
-    past_bc = jnp.concatenate(
-        [
-            jnp.sum(window_bc_v[s].astype(F32) * conv_bcf[: taps - 1], axis=0, keepdims=True)
-            for s in range(seqs)
-        ],
-        axis=0,
-    )
+    past_x = sum(window_x_v[j].astype(F32) * conv_xf[j : j + 1] for j in range(taps - 1))
+    past_pairs = [
+        sum(window_bc_v[s, j].astype(F32) * conv_bc_v[j].astype(F32) for j in range(taps - 1))
+        for s in range(seqs)
+    ]
+
+    def side_by_side(pairs):
+        return jnp.concatenate(
+            [jnp.concatenate([p[h : h + 1] for p in pairs], axis=0) for h in range(2)], axis=1
+        )
+
+    past_bc = side_by_side(past_pairs)
+    last_bc = side_by_side([conv_bc_v[taps - 1].astype(F32)])
+    for j in range(1, taps - 1):
+        new_x_out[j - 1] = window_x_v[j]
+        for s in range(seqs):
+            new_bc_out[s, j - 1] = window_bc_v[s, j]
     state_half[...] = state_v[...].astype(BF16)
     lanes = lax.broadcasted_iota(jnp.int32, (heads, inner), 1)
     owner = lax.broadcasted_iota(jnp.int32, (heads, inner), 0)
@@ -387,6 +396,8 @@
     skip = expand(jnp.broadcast_to(skip_v[...], (8, heads)))[:seqs]
     for copy in proj_copies:
         copy.wait()
+    for half in range(2):
+        bc_halves[half] = bc_v[:, half, :]
 
     for offset in range(1, n):
         peer, _, _ = peer_of(offset)
@@ -401,12 +412,17 @@
     squares = jnp.sum(after32 * after32, axis=1, keepdims=True)
     gain_part = gain_m_v[:, pl.ds(pl.multiple_of(kv * kv_cols, 128), kv_cols)]
     scaled = (after32 * gain_part).astype(BF16)
-    own_rates = dot32(scaled, dt_v[...])
+    own_rates = dot32_rows(scaled, dt_v[...])
     for k in range(n_kv):
         rows_k = slice(k * seqs, (k + 1) * seqs)
         extra_send[k] = jnp.broadcast_to(squares[rows_k], (seqs, extra_send.shape[2]))
         extra_send[k, :, :heads] = own_rates[rows_k]
-    for place, weight in ((0, z_v), (inner, x_v), (2 * inner, bc_v)):
+    for place, weight in (
+        (0, z_v),
+        (inner, x_v),
+        (2 * inner, bc_halves.at[0]),
+        (2 * inner + group_width, bc_halves.at[1]),
+    ):
         piece = dot32(scaled, weight[...])
         for k in range(n_kv):
             proj_send[k, :, pl.ds(place, weight.shape[1])] = piece[
@@ -440,7 +456,7 @@
     x_new = projected[:, inner : 2 * inner].astype(BF16)
     bc_new = projected[:, 2 * inner :].astype(BF16)
     mixed_x = jax.nn.silu(past_x + conv_xf[taps - 1 :] * x_new.astype(F32))
-    mixed_bc = jax.nn.silu(past_bc + conv_bcf[taps - 1 :] * bc_new.astype(F32))
+    mixed_bc = jax.nn.silu(past_bc + last_bc * bc_new.astype(F32))
     step_x = expand(step_size) * mixed_x
     retained = expand(retain)
     pieces = []
@@ -469,10 +485,14 @@
         to_kv = lax.rem(kv + step, n_kv)
         send(mixed_all.at[kv], mixed_all.at[kv], MIXED, step, kv, to_kv, tp)
     step_x_out[...] = step_x
-    retain_out[...] = retain
+    retain_out[...] = retained
     b_out[...] = mixed_bc[:, :group_width]
-    x_new_out[...] = x_new
-    bc_new_out[...] = bc_new
+    new_x_out[taps - 2] = x_new
+    bc32 = bc_new.astype(F32)
+    for s in range(seqs):
+        new_bc_out[s, taps - 2] = jnp.concatenate(
+            [bc32[s : s + 1, :group_width], bc32[s : s + 1, group_width:]], axis=0
+        ).astype(BF16)
     out_copy.wait()
     for step in range(1, n_kv):
         from_kv = lax.rem(kv + step, n_kv)
@@ -525,6 +545,47 @@
     result[...] = (mine + 0.5 * summed).astype(BF16)
     for copy in sends:
         copy.wait_send()
+
+
+def finish_kernel(
+    result,
+    step_x,
+    retain,
+    keys_b,
+    new_x,
+    new_bc,
+    state,
+    result_out,
+    state_out,
+    new_x_out,
+    new_bc_out,
+    fresh,
+    sems,
+):
+    seqs, inner, state_size = state.shape
+    groups = keys_b.shape[1] // state_size
+    span = inner // groups
+    rows = jnp.concatenate([retain[...], step_x[...], retain[...], step_x[...]], axis=0)
+    columns = rows.T
+    copies = []
+    for g in range(groups):
+        part = slice(g * span, (g + 1) * span)
+        for s in range(seqs):
+            fresh[s, part, :] = (
+                columns[part, s : s + 1] * state[s, part, :]
+                + columns[part, seqs + s : seqs + s + 1]
+                * keys_b[s : s + 1, g * state_size : (g + 1) * state_size]
+            )
+            copy = pltpu.make_async_copy(
+                fresh.at[s, part], state_out.at[s, part], sems.at[s, g]
+            )
+            copy.start()
+            copies.append(copy)
+    result_out[...] = result[...]
+    new_x_out[...] = new_x[...]
+    new_bc_out[...] = new_bc[...]
+    for copy in copies:
+        copy.wait()
 
 
 def per_device(n_kv, n_tp, *args):
@@ -567,18 +628,18 @@
     operands = (
         tokens,
         mlp1_gain[None],
-        mlp1_gate,
-        mlp1_up,
+        mlp1_gate.T,
+        mlp1_up.T,
         mlp1_down,
         mixer_gain[None],
         proj_z,
         proj_x,
-        proj_bc.reshape(proj_bc.shape[0], 2 * group_width),
-        proj_dt,
+        proj_bc,
+        proj_dt.T,
         conv_x,
-        conv_bc.reshape(taps, 2 * group_width),
-        window_x,
-        window_bc.reshape(seqs, taps - 1, 2 * group_width),
+        conv_bc,
+        jnp.swapaxes(window_x, 0, 1),
+        window_bc,
         ssm_state.reshape(seqs, inner, state_size),
         dt_bias[None],
         log_rate[None],
@@ -586,13 +647,14 @@
         group_gain[None],
         out_weight,
         mlp2_gain[None],
-        mlp2_gate,
-        mlp2_up,
+        mlp2_gate.T,
+        mlp2_up.T,
         mlp2_down,
     )
     vmem = [pltpu.VMEM(a.shape, a.dtype) for a in operands]
     scratch = vmem + [
         pltpu.VMEM((seqs, inner, state_size), BF16),
+        pltpu.VMEM((2, proj_bc.shape[0], group_width), BF16),
         pltpu.VMEM((n, rows, cols), BF16),
         pltpu.VMEM((n_kv, rows, kv_cols), BF16),
         pltpu.VMEM((n, rows, kv_cols), BF16),
@@ -612,12 +674,12 @@
     shapes = (
         jax.ShapeDtypeStruct((rows, cols), BF16),
         jax.ShapeDtypeStruct((seqs, inner), F32),
-        jax.ShapeDtypeStruct((seqs, heads), F32),
+        jax.ShapeDtypeStruct((seqs, inner), F32),
         jax.ShapeDtypeStruct((seqs, group_width), F32),
-        jax.ShapeDtypeStruct((seqs, inner), BF16),
-        jax.ShapeDtypeStruct((seqs, 2 * group_width), BF16),
-    )
-    result, step_x, retain, keys_b, x_new, bc_new = pl.pallas_call(
+        jax.ShapeDtypeStruct((taps - 1, seqs, inner), BF16),
+        jax.ShapeDtypeStruct(window_bc.shape, BF16),
+    )
+    result, step_x, retain, keys_b, new_x, new_bc = pl.pallas_call(
         functools.partial(fused_kernel, n_kv, n_tp),
         out_shape=shapes,
         in_specs=[pl.BlockSpec(memory_space=pl.ANY)] * len(operands),
@@ -627,16 +689,23 @@
             collective_id=0, has_side_effects=True, vmem_limit_bytes=60 * 1024 * 1024
         ),
     )(*operands)
-    keys_b = jnp.repeat(keys_b.reshape(seqs, groups, state_size), heads // groups, axis=1)
-    new_state = (
-        retain[:, :, None, None] * ssm_state
-        + step_x.reshape(seqs, heads, inner // heads)[:, :, :, None] * keys_b[:, :, None, :]
-    )
-    new_x = jnp.concatenate([window_x[:, 1:], x_new[:, None]], axis=1)
-    new_bc = jnp.concatenate(
-        [window_bc[:, 1:], bc_new.reshape(seqs, 1, 2, group_width)], axis=1
-    )
-    return (result, new_state, new_x, new_bc)
+    whole = pl.BlockSpec(memory_space=pltpu.VMEM)
+    result, new_state, new_x, new_bc = pl.pallas_call(
+        finish_kernel,
+        out_shape=(
+            shapes[0],
+            jax.ShapeDtypeStruct(operands[14].shape, F32),
+            shapes[4],
+            shapes[5],
+        ),
+        in_specs=[whole] * 7,
+        out_specs=(whole, pl.BlockSpec(memory_space=pl.ANY), whole, whole),
+        scratch_shapes=[
+            pltpu.VMEM(operands[14].shape, F32),
+            pltpu.SemaphoreType.DMA((seqs, groups)),
+        ],
+    )(result, step_x, retain, keys_b, new_x, new_bc, operands[14])
+    return (result, new_state.reshape(ssm_state.shape), jnp.swapaxes(new_x, 0, 1), new_bc)
 
 
 def solution(mesh):

time: 60.5 us -> 39.4 us (0.65)
  local copies, waits for them, and re-layouts: 22.1 us -> 0 us
  Pallas kernels: 33.5 us -> 38.5 us
  other arithmetic: 3.87 us -> 0 us
    unnamed x25 -> x0, local copies, waits for them, and re-layouts: 19.4 us -> none
    pallas_call x0 -> x1, Pallas kernels: none -> 3.56 us  [per_device(): pl.pallas_call(finish_kernel, out_shape=(shapes[0], jax.ShapeDtypeStruct(...]
    add x1 -> x0, other arithmetic: 1.98 us -> none  [per_device(): retain[:, :, None, None] * ssm_state]
    reshape x3 -> x0, local copies, waits for them, and re-layouts: 1.93 us -> none  [the longest x1 0.69 us: per_device(): keys_b.reshape(seqs, groups, state_size)]
    concatenate x2 -> x0, other arithmetic: 1.9 us -> none  [the longest x1 1.29 us: per_device(): new_x = jnp.concatenate([window_x[:, 1:], x_new[:, None]], axis=1)]
    pallas_call x1, Pallas kernels: 33.5 us -> 35 us  [per_device(): pl.pallas_call(functools.partial(fused_kernel, n_kv, n_tp), out_shape=sha...]
    mul x2 -> x0, local copies, waits for them, and re-layouts: 0.78 us -> none  [per_device(): step_x.reshape(seqs, heads, inner // heads)[:, :, :, None]]
where the time goes in v2:
time: 39.4 us; the launch traced here: 39.2 us
  Pallas kernels  38.5 us (98%)
  between operations  0.65 us (2%)
    pallas_call x1, Pallas kernels, per_device(): pl.pallas_call(functools.partial(fused_kernel, n_kv, n_tp), out_shape=sha...  35 us
    pallas_call x1, Pallas kernels, per_device(): pl.pallas_call(finish_kernel, out_shape=(shapes[0], jax.ShapeDtypeStruct(...  3.56 us

profile of v2, /device:TPU:0, one launch (start us, length us, event | category | flops | bytes accessed | tf_op | source)
XLA Modules:
  0.0 39.2 jit_solution(15986952514309601791)
XLA Ops:
  0.6 35.0 %shard_map.255 = (bf16[8,256]{1,0:T(8,128)(2,1)}, f32[2,1024]{1,0:T(2,128)}, f32[2,1024]{1,0:T(2,128)}, f32[2,256]{1,0:T(2,128)}, bf16[3,2,1024]{2,1,0:T(2,128)(2,1)}, /*index=5*/bf16[2,3,2,256]{3,2,1,0:T(2,128)(2,1)}) custom-call(bf16[8,256]{1,0:T(8,128)(2,1)} %tokens.1, f32[1,2048]{1,0:T(1,128)} %bitcast.24, bf16[704,2048]{1,0:T(8,128)(2,1)} %bitcast.18, ...), custom_call_target="tpu_custom_call" | custom-call | tf_op jit(solution)/shard_map/pallas_call | solution.py:682
  35.6 3.6 %shard_map.256 = (bf16[8,256]{1,0:T(8,128)(2,1)}, f32[2,1024,128]{2,1,0:T(8,128)}, bf16[3,2,1024]{2,1,0:T(2,128)(2,1)}, bf16[2,3,2,256]{3,2,1,0:T(2,128)(2,1)}) custom-call(bf16[8,256]{1,0:T(8,128)(2,1)} %get-tuple-element.14.result, f32[2,1024]{1,0:T(2,128)} %get-tuple-element.15.step_x, f32[2,1024]{1,0:T(2,128)} %get-tuple-element.16.retain, ...), custom_call_target="tpu_custom_call" | custom-call | tf_op jit(solution)/shard_map/pallas_call | solution.py:693

commit v3 on v2

--- a/solution.py
+++ b/solution.py
@@ -211,6 +211,12 @@
     out_all,
     sum2_send,
     sum2_all,
+    result_v,
+    step_x_v,
+    retain_v,
+    b_v,
+    new_x_v,
+    new_bc_v,
     local_sem,
     send_sem,
     recv_sem,
@@ -229,11 +235,23 @@
         copy.start()
         return copy
 
-    chunk = cols
+    def nth_kv(i):
+        down = n_kv - 1 - i
+        down = down - lax.div(kv - down + n_kv, n_kv)
+        up = i + lax.div(i - kv + n_kv, n_kv)
+        half = lax.div(2 * kv, n_kv)
+        return down * (1 - half) + up * half
+
+    far_kv = [nth_kv(i) for i in range(n_kv - 1)]
+    others_tp = [lax.rem(tp + t, n_tp) for t in range(1, n_tp)]
+    all_tp = [tp] + others_tp
+    far_peers = [(k, t) for k in far_kv for t in all_tp] + [(kv, t) for t in others_tp]
+    near_first = [(kv, tp)] + far_peers[::-1]
+
     tok_copies = [load(tokens, tok_v), load(gain1, gain1_v)]
     gu1 = []
-    for i in range(n):
-        part = pl.ds(i * chunk, chunk)
+    for k, t in near_first:
+        part = pl.ds(pl.multiple_of((k * n_tp + t) * cols, 128), cols)
         gu1.append(
             (load(gate1.at[:, part], gate1_v.at[:, part]), load(up1.at[:, part], up1_v.at[:, part]))
         )
@@ -261,16 +279,9 @@
     gu2 = [load(gate2, gate2_v), load(up2, up2_v)]
     down2_copy = load(down2, down2_v)
 
-    def peer_of(offset):
-        peer = lax.rem(me + offset, n)
-        return peer, lax.div(peer, n_tp), lax.rem(peer, n_tp)
-
     barrier = pltpu.get_barrier_semaphore()
-    for offset in range(1, n):
-        _, peer_kv, peer_tp = peer_of(offset)
-        pl.semaphore_signal(
-            barrier, inc=1, device_id={"kv": peer_kv, "tp": peer_tp}, device_id_type=MESH
-        )
+    for k, t in far_peers:
+        pl.semaphore_signal(barrier, inc=1, device_id={"kv": k, "tp": t}, device_id_type=MESH)
     pl.semaphore_wait(barrier, n - 1)
 
     sends = []
@@ -299,59 +310,45 @@
 
     for copy in tok_copies:
         copy.wait()
-    for offset in range(1, n):
-        _, peer_kv, peer_tp = peer_of(offset)
-        send(tok_v, tok_all.at[me], TOKENS, offset, me, peer_kv, peer_tp)
+    for i, (k, t) in enumerate(far_peers):
+        send(tok_v, tok_all.at[me], TOKENS, i, me, k, t)
     tok_all[me] = tok_v[...]
-    for offset in range(1, n):
-        peer, _, _ = peer_of(offset)
-        arrive(tok_all.at[peer], TOKENS, peer)
-
-    def hidden_of(parts, gain_ref, gate_ref, up_ref, ready):
-        squares = sum(jnp.sum(v * v, axis=1, keepdims=True) for v in parts)
-        factor = lax.rsqrt(squares / width + EPS)
-        gate_part = up_part = None
-        for i, v in enumerate(parts):
+
+    def hidden_of(sources, value_of, gain_ref, gate_ref, up_ref):
+        squares = gate_part = up_part = None
+        for i, source in enumerate(sources):
+            index, v = value_of(i, source)
             piece = v.shape[1]
-            part = pl.ds(i * piece, piece)
-            normed = (v * factor * gain_ref[:, part]).astype(BF16)
-            ready(i)
-            a, b = dot32_rows(normed, gate_ref[:, part]), dot32_rows(normed, up_ref[:, part])
+            part = pl.ds(pl.multiple_of(index * piece, 128), piece)
+            scaled_v = (v * gain_ref[:, part]).astype(BF16)
+            q = jnp.sum(v * v, axis=1, keepdims=True)
+            a = dot32_rows(scaled_v, gate_ref[:, part])
+            b = dot32_rows(scaled_v, up_ref[:, part])
+            squares = q if i == 0 else squares + q
             gate_part = a if i == 0 else gate_part + a
             up_part = b if i == 0 else up_part + b
-        return (jax.nn.silu(gate_part) * up_part).astype(BF16)
-
-    def ready1(i):
+        factor = lax.rsqrt(squares / width + EPS)
+        return (jax.nn.silu(gate_part * factor) * (up_part * factor)).astype(BF16)
+
+    def token_block(i, source):
+        peer = source[0] * n_tp + source[1]
+        if i:
+            arrive(tok_all.at[peer], TOKENS, peer)
         for copy in gu1[i]:
             copy.wait()
-
-    hidden1 = hidden_of(
-        [tok_all[i].astype(F32) for i in range(n)], gain1_v, gate1_v, up1_v, ready1
-    )
+        return peer, (tok_all[peer] if i else tok_v[...]).astype(F32)
+
+    hidden1 = hidden_of(near_first, token_block, gain1_v, gate1_v, up1_v)
     down1_copy.wait()
-    for step in range(1, n_kv + 1):
-        to_kv = lax.rem(kv + step, n_kv)
+    for i, to_kv in enumerate(far_kv + [kv]):
         part = pl.ds(pl.multiple_of(to_kv * kv_cols, 128), kv_cols)
         partial_sum = dot32(hidden1, down1_v[:, part]).astype(BF16)
-        if step < n_kv:
-            sum1_send[step] = partial_sum
-            for other in range(n_tp):
-                to_tp = lax.rem(tp + other, n_tp)
-                send(
-                    sum1_send.at[step],
-                    sum1_all.at[me],
-                    SUM1,
-                    step * n_tp + other,
-                    me,
-                    to_kv,
-                    to_tp,
-                )
-        else:
+        sum1_send[i] = partial_sum
+        if i == n_kv - 1:
             sum1_all[me] = partial_sum
-            sum1_send[0] = partial_sum
-            for other in range(1, n_tp):
-                to_tp = lax.rem(tp + other, n_tp)
-                send(sum1_send.at[0], sum1_all.at[me], SUM1, other, me, kv, to_tp)
+        for j, to_tp in enumerate(all_tp):
+            if i < n_kv - 1 or j:
+                send(sum1_send.at[i], sum1_all.at[me], SUM1, i * n_tp + j, me, to_kv, to_tp)
 
     for copy in ssm_copies:
         copy.wait()
@@ -379,9 +376,9 @@
     past_bc = side_by_side(past_pairs)
     last_bc = side_by_side([conv_bc_v[taps - 1].astype(F32)])
     for j in range(1, taps - 1):
-        new_x_out[j - 1] = window_x_v[j]
+        new_x_v[j - 1] = window_x_v[j]
         for s in range(seqs):
-            new_bc_out[s, j - 1] = window_bc_v[s, j]
+            new_bc_v[s, j - 1] = window_bc_v[s, j]
     state_half[...] = state_v[...].astype(BF16)
     lanes = lax.broadcasted_iota(jnp.int32, (heads, inner), 1)
     owner = lax.broadcasted_iota(jnp.int32, (heads, inner), 0)
@@ -399,9 +396,8 @@
     for half in range(2):
         bc_halves[half] = bc_v[:, half, :]
 
-    for offset in range(1, n):
-        peer, _, _ = peer_of(offset)
-        arrive(sum1_all.at[peer], SUM1, peer)
+    for k, t in far_peers:
+        arrive(sum1_all.at[k * n_tp + t], SUM1, k * n_tp + t)
     summed = sum1_all[0].astype(F32)
     for i in range(1, n):
         summed = summed + sum1_all[i].astype(F32)
@@ -430,16 +426,13 @@
             ].astype(BF16)
     proj_all[kv] = proj_send[kv]
     extra_all[kv] = extra_send[kv]
-    for step in range(1, n_kv):
-        to_kv = lax.rem(kv + step, n_kv)
+    for step, to_kv in enumerate(far_kv):
         send(proj_send.at[to_kv], proj_all.at[kv], PROJ, step, kv, to_kv, tp)
         send(extra_send.at[to_kv], extra_all.at[kv], EXTRA, step, kv, to_kv, tp)
-    for step in range(1, n_kv):
-        to_kv = lax.rem(kv + step, n_kv)
+    for step, to_kv in enumerate(far_kv):
         send(first_all.at[kv], first_all.at[kv], FIRST, step, kv, to_kv, tp)
 
-    for step in range(1, n_kv):
-        from_kv = lax.rem(kv + step, n_kv)
+    for from_kv in far_kv:
         arrive(extra_all.at[from_kv], EXTRA, from_kv)
         arrive(proj_all.at[from_kv], PROJ, from_kv)
     extra = extra_all[0]
@@ -481,38 +474,36 @@
         gated = gated * lax.rsqrt(jnp.mean(gated * gated, axis=1, keepdims=True) + EPS)
         pieces.append((gated * ggain_v[:, span]).astype(BF16))
     mixed_all[kv] = jnp.concatenate(pieces, axis=1)
-    for step in range(1, n_kv):
-        to_kv = lax.rem(kv + step, n_kv)
+    for step, to_kv in enumerate(far_kv):
         send(mixed_all.at[kv], mixed_all.at[kv], MIXED, step, kv, to_kv, tp)
-    step_x_out[...] = step_x
-    retain_out[...] = retained
-    b_out[...] = mixed_bc[:, :group_width]
-    new_x_out[taps - 2] = x_new
+    step_x_v[...] = step_x
+    retain_v[...] = retained
+    b_v[...] = mixed_bc[:, :group_width]
+    new_x_v[taps - 2] = x_new
     bc32 = bc_new.astype(F32)
     for s in range(seqs):
-        new_bc_out[s, taps - 2] = jnp.concatenate(
+        new_bc_v[s, taps - 2] = jnp.concatenate(
             [bc32[s : s + 1, :group_width], bc32[s : s + 1, group_width:]], axis=0
         ).astype(BF16)
+    out_copies = [
+        load(step_x_v, step_x_out),
+        load(retain_v, retain_out),
+        load(b_v, b_out),
+        load(new_x_v, new_x_out),
+        load(new_bc_v, new_bc_out),
+    ]
     out_copy.wait()
-    for step in range(1, n_kv):
-        from_kv = lax.rem(kv + step, n_kv)
+    for from_kv in far_kv:
         arrive(mixed_all.at[from_kv], MIXED, from_kv)
     mixed = jnp.concatenate([mixed_all[k].astype(F32) for k in range(n_kv)], axis=0)
     out_all[me] = dot32(mixed.astype(BF16), out_v[...]).astype(BF16)
-    for offset in range(1, n):
-        _, peer_kv, peer_tp = peer_of(offset)
-        send(out_all.at[me], out_all.at[me], OUT, offset, me, peer_kv, peer_tp)
+    for i, (k, t) in enumerate(far_peers):
+        send(out_all.at[me], out_all.at[me], OUT, i, me, k, t)
 
     gain2_copy.wait()
     for copy in gu2:
         copy.wait()
     down2_copy.wait()
-    for step in range(1, n_kv):
-        from_kv = lax.rem(kv + step, n_kv)
-        arrive(first_all.at[from_kv], FIRST, from_kv)
-    for offset in range(1, n):
-        peer, _, _ = peer_of(offset)
-        arrive(out_all.at[peer], OUT, peer)
 
     def after_of(k):
         total = out_all[k * n_tp].astype(F32)
@@ -520,31 +511,40 @@
             total = total + out_all[k * n_tp + t].astype(F32)
         return (first_all[k].astype(F32) + total).astype(BF16).astype(F32)
 
-    hidden2 = hidden_of(
-        [after_of(k) for k in range(n_kv)], gain2_v, gate2_v, up2_v, lambda i: None
-    )
-    for offset in range(1, n + 1):
-        peer, peer_kv, peer_tp = peer_of(offset)
-        part = pl.ds(pl.multiple_of(peer * cols, 128), cols)
+    def mixer_block(i, k):
+        for t in all_tp if i else others_tp:
+            arrive(out_all.at[k * n_tp + t], OUT, k * n_tp + t)
+        if i:
+            arrive(first_all.at[k], FIRST, k)
+        return k, after_of(k)
+
+    hidden2 = hidden_of([kv] + far_kv[::-1], mixer_block, gain2_v, gate2_v, up2_v)
+    for i, to_kv in enumerate(far_kv + [kv]):
+        part = pl.ds(pl.multiple_of(to_kv * kv_cols, 128), kv_cols)
         partial_sum = dot32(hidden2, down2_v[:, part]).astype(BF16)
-        if offset < n:
-            sum2_send[offset] = partial_sum
-            send(sum2_send.at[offset], sum2_all.at[me], SUM2, offset, me, peer_kv, peer_tp)
-        else:
-            sum2_all[me] = partial_sum
+        for t in range(n_tp):
+            sum2_send[i, t] = partial_sum[:, t * cols : (t + 1) * cols]
+        for j, to_tp in enumerate(all_tp):
+            if i < n_kv - 1 or j:
+                send(
+                    sum2_send.at[i, to_tp], sum2_all.at[me], SUM2, i * n_tp + j, me, to_kv, to_tp
+                )
+    sum2_all[me] = sum2_send[n_kv - 1, tp]
     own = after_of(kv)
     mine = own[:, :cols]
     for t in range(1, n_tp):
         mine = jnp.where(tp == t, own[:, t * cols : (t + 1) * cols], mine)
-    for offset in range(1, n):
-        peer, _, _ = peer_of(offset)
-        arrive(sum2_all.at[peer], SUM2, peer)
+    for k, t in far_peers:
+        arrive(sum2_all.at[k * n_tp + t], SUM2, k * n_tp + t)
     summed = sum2_all[0].astype(F32)
     for i in range(1, n):
         summed = summed + sum2_all[i].astype(F32)
-    result[...] = (mine + 0.5 * summed).astype(BF16)
+    result_v[...] = (mine + 0.5 * summed).astype(BF16)
+    out_copies.append(load(result_v, result))
     for copy in sends:
         copy.wait_send()
+    for copy in out_copies:
+        copy.wait()
 
 
 def finish_kernel(
@@ -559,32 +559,65 @@
     state_out,
     new_x_out,
     new_bc_out,
+    result_v,
+    step_x_v,
+    retain_v,
+    b_v,
+    new_x_v,
+    new_bc_v,
+    old,
     fresh,
-    sems,
+    in_sem,
+    out_sem,
+    old_sem,
+    fresh_sem,
 ):
     seqs, inner, state_size = state.shape
     groups = keys_b.shape[1] // state_size
     span = inner // groups
-    rows = jnp.concatenate([retain[...], step_x[...], retain[...], step_x[...]], axis=0)
+
+    def start(source, target, sem):
+        copy = pltpu.make_async_copy(source, target, sem)
+        copy.start()
+        return copy
+
+    needed = [
+        start(step_x, step_x_v, in_sem.at[0]),
+        start(retain, retain_v, in_sem.at[1]),
+        start(keys_b, b_v, in_sem.at[2]),
+    ]
+    blocks = [
+        (s, g, pl.ds(g * span, span)) for g in range(groups) for s in range(seqs)
+    ]
+    reads = [start(state.at[s, part], old.at[s, part], old_sem.at[s, g]) for s, g, part in blocks]
+    passed = [
+        (start(source, held, in_sem.at[3 + i]), held, target)
+        for i, (source, held, target) in enumerate(
+            (
+                (result, result_v, result_out),
+                (new_x, new_x_v, new_x_out),
+                (new_bc, new_bc_v, new_bc_out),
+            )
+        )
+    ]
+    for copy in needed:
+        copy.wait()
+    rows = jnp.concatenate([retain_v[...], step_x_v[...]] * (8 // (2 * seqs)), axis=0)
     columns = rows.T
-    copies = []
-    for g in range(groups):
-        part = slice(g * span, (g + 1) * span)
-        for s in range(seqs):
-            fresh[s, part, :] = (
-                columns[part, s : s + 1] * state[s, part, :]
-                + columns[part, seqs + s : seqs + s + 1]
-                * keys_b[s : s + 1, g * state_size : (g + 1) * state_size]
-            )
-            copy = pltpu.make_async_copy(
-                fresh.at[s, part], state_out.at[s, part], sems.at[s, g]
-            )
-            copy.start()
-            copies.append(copy)
-    result_out[...] = result[...]
-    new_x_out[...] = new_x[...]
-    new_bc_out[...] = new_bc[...]
-    for copy in copies:
+    writes = []
+    for read, (s, g, part) in zip(reads, blocks):
+        read.wait()
+        here = slice(g * span, (g + 1) * span)
+        fresh[s, part, :] = (
+            columns[here, s : s + 1] * old[s, part, :]
+            + columns[here, seqs + s : seqs + s + 1]
+            * b_v[s : s + 1, g * state_size : (g + 1) * state_size]
+        )
+        writes.append(start(fresh.at[s, part], state_out.at[s, part], fresh_sem.at[s, g]))
+    for i, (copy, held, target) in enumerate(passed):
+        copy.wait()
+        writes.append(start(held, target, out_sem.at[i]))
+    for copy in writes:
         copy.wait()
 
 
@@ -616,7 +649,7 @@
         mlp2_down,
     ) = args
     rows, cols = tokens.shape
-    if cols % 128 or n_kv * n_tp > 16 or rows % 8:
+    if cols % 128 or n_kv * n_tp > 16 or rows % 8 or 8 % (2 * window_x.shape[0]):
         return plain_device(*args)
     n = n_kv * n_tp
     kv_cols = cols * n_tp
@@ -665,11 +698,8 @@
         pltpu.VMEM((n_kv, rows, kv_cols), BF16),
         pltpu.VMEM((n_kv, seqs, inner), BF16),
         pltpu.VMEM((n, rows, kv_cols), BF16),
+        pltpu.VMEM((n_kv, n_tp, rows, cols), BF16),
         pltpu.VMEM((n, rows, cols), BF16),
-        pltpu.VMEM((n, rows, cols), BF16),
-        pltpu.SemaphoreType.DMA((2 * n + 40,)),
-        pltpu.SemaphoreType.DMA((PHASES, n)),
-        pltpu.SemaphoreType.DMA((PHASES, n)),
     ]
     shapes = (
         jax.ShapeDtypeStruct((rows, cols), BF16),
@@ -679,32 +709,44 @@
         jax.ShapeDtypeStruct((taps - 1, seqs, inner), BF16),
         jax.ShapeDtypeStruct(window_bc.shape, BF16),
     )
+    scratch += [pltpu.VMEM(a.shape, a.dtype) for a in shapes]
+    scratch += [
+        pltpu.SemaphoreType.DMA((2 * n + 40,)),
+        pltpu.SemaphoreType.DMA((PHASES, n)),
+        pltpu.SemaphoreType.DMA((PHASES, n)),
+    ]
+    anywhere = pl.BlockSpec(memory_space=pl.ANY)
+    small, state_flat = shapes, operands[14]
     result, step_x, retain, keys_b, new_x, new_bc = pl.pallas_call(
         functools.partial(fused_kernel, n_kv, n_tp),
         out_shape=shapes,
-        in_specs=[pl.BlockSpec(memory_space=pl.ANY)] * len(operands),
-        out_specs=[pl.BlockSpec(memory_space=pltpu.VMEM)] * len(shapes),
+        in_specs=[anywhere] * len(operands),
+        out_specs=[anywhere] * len(shapes),
         scratch_shapes=scratch,
         compiler_params=pltpu.CompilerParams(
             collective_id=0, has_side_effects=True, vmem_limit_bytes=60 * 1024 * 1024
         ),
     )(*operands)
-    whole = pl.BlockSpec(memory_space=pltpu.VMEM)
     result, new_state, new_x, new_bc = pl.pallas_call(
         finish_kernel,
         out_shape=(
             shapes[0],
-            jax.ShapeDtypeStruct(operands[14].shape, F32),
+            jax.ShapeDtypeStruct(state_flat.shape, F32),
             shapes[4],
             shapes[5],
         ),
-        in_specs=[whole] * 7,
-        out_specs=(whole, pl.BlockSpec(memory_space=pl.ANY), whole, whole),
-        scratch_shapes=[
-            pltpu.VMEM(operands[14].shape, F32),
+        in_specs=[anywhere] * 7,
+        out_specs=[anywhere] * 4,
+        scratch_shapes=[pltpu.VMEM(a.shape, a.dtype) for a in small]
+        + [
+            pltpu.VMEM(state_flat.shape, F32),
+            pltpu.VMEM(state_flat.shape, F32),
+            pltpu.SemaphoreType.DMA((6,)),
+            pltpu.SemaphoreType.DMA((3,)),
+            pltpu.SemaphoreType.DMA((seqs, groups)),
             pltpu.SemaphoreType.DMA((seqs, groups)),
         ],
-    )(result, step_x, retain, keys_b, new_x, new_bc, operands[14])
+    )(result, step_x, retain, keys_b, new_x, new_bc, state_flat)
     return (result, new_state.reshape(ssm_state.shape), jnp.swapaxes(new_x, 0, 1), new_bc)
 
 

time: 39.4 us -> 35 us (0.89)
  Pallas kernels: 38.5 us -> 34.2 us
    pallas_call x1, Pallas kernels: 35 us -> 31.5 us  [per_device(): pl.pallas_call(functools.partial(fused_kernel, n_kv, n_tp), out_shape=sha...]
    pallas_call x1, Pallas kernels: 3.56 us -> 2.67 us  [per_device(): pl.pallas_call(finish_kernel, out_shape=(shapes[0], jax.ShapeDtypeStruct(...]
where the time goes in v3:
time: 35 us; the launch traced here: 34.8 us
  Pallas kernels  34.2 us (98%)
  between operations  0.65 us (2%)
    pallas_call x1, Pallas kernels, per_device(): pl.pallas_call(functools.partial(fused_kernel, n_kv, n_tp), out_shape=sha...  31.5 us
    pallas_call x1, Pallas kernels, per_device(): pl.pallas_call(finish_kernel, out_shape=(shapes[0], jax.ShapeDtypeStruct(...  2.67 us

profile of v3, /device:TPU:0, one launch (start us, length us, event | category | flops | bytes accessed | tf_op | source)
XLA Modules:
  0.0 34.8 jit_solution(306515596254854949)
XLA Ops:
  0.6 31.5 %shard_map.255 = (bf16[8,256]{1,0:T(8,128)(2,1)}, f32[2,1024]{1,0:T(2,128)}, f32[2,1024]{1,0:T(2,128)}, f32[2,256]{1,0:T(2,128)}, bf16[3,2,1024]{2,1,0:T(2,128)(2,1)}, /*index=5*/bf16[2,3,2,256]{3,2,1,0:T(2,128)(2,1)}) custom-call(bf16[8,256]{1,0:T(8,128)(2,1)} %tokens.1, f32[1,2048]{1,0:T(1,128)} %bitcast.24, bf16[704,2048]{1,0:T(8,128)(2,1)} %bitcast.18, ...), custom_call_target="tpu_custom_call" | custom-call | tf_op jit(solution)/shard_map/pallas_call | solution.py:720
  32.2 2.7 %shard_map.256 = (bf16[8,256]{1,0:T(8,128)(2,1)}, f32[2,1024,128]{2,1,0:T(8,128)}, bf16[3,2,1024]{2,1,0:T(2,128)(2,1)}, bf16[2,3,2,256]{3,2,1,0:T(2,128)(2,1)}) custom-call(bf16[8,256]{1,0:T(8,128)(2,1)} %get-tuple-element.14.result, f32[2,1024]{1,0:T(2,128)} %get-tuple-element.15.step_x, f32[2,1024]{1,0:T(2,128)} %get-tuple-element.16.retain, ...), custom_call_target="tpu_custom_call" | custom-call | tf_op jit(solution)/shard_map/pallas_call | solution.py:730
